TPU v7x, 256 devices: a whole 4x4x8 slice. The times are simulated.
256 devices in a mesh: ep: 32 (over z, x), tp: 8 (over y, core).
Axes of the slice: x: 4, y: 4, z: 8, core: 2. Of those that a mesh axis runs over, the one named last changes fastest.
Arguments:
- tokens: bfloat16 [2048, 2048], P('ep', 'tp')
- norm_gain: float32 [2048], P('tp'), may hold values from 0.1 to 1.9
- expert_ids: int32 [2048, 4], P('ep'), may hold values from 0 to 31, all different within a row; in each aligned block of 64 rows (0 to 63, 64 to 127, ...) at most 16 rows name the same one
- route_weights: float32 [2048, 4], P('ep'), may hold values from 0.1 to 1
- gate_proj: bfloat16 [32, 2048, 2048], P('ep', None, 'tp'), may hold values from -0.5 to 0.5
- up_proj: bfloat16 [32, 2048, 2048], P('ep', None, 'tp'), may hold values from -0.5 to 0.5
- down_proj: bfloat16 [32, 2048, 2048], P('ep', 'tp')
- final_gain: float32 [2048], P('tp'), may hold values from 0.1 to 1.9
Outputs:
- layer_output: bfloat16 [2048, 2048], P('ep', 'tp')
Inputs may be any that keep to these rules, and one draw needn't show every extreme that they name: `expert_ids`: each row names 4 different experts. Within the 64 rows of one device no expert is named by more than 16 rows, a bound that some block reaches.
All inputs are finite; a program needn't handle non-finite values.
Results may differ from a plain program's by a relative error of at most 0.017.
Values may be sent and summed in bfloat16 or wider, within the bound.
A program may use at most 64 MiB of HBM per device.

v0:
```python
import jax
import jax.numpy as jnp
from jax import lax
from jax.sharding import PartitionSpec as P

EPSILON = 1e-05
CLAMP_LIMIT = 7.0
SIGMOID_SLOPE = 1.702


def from_everyone(shard, axis):
    peers = lax.axis_size(axis)
    return lax.all_to_all(
        jnp.broadcast_to(shard[None], (peers, *shard.shape)), axis, 0, 0, tiled=True
    )


def over_copies(shard, axis):
    everything = from_everyone(shard, axis)
    return jnp.sum(everything, axis=0)


def split_up(shard, dim, peers):
    dims = shard.shape
    blocks = shard.reshape(*dims[:dim], peers, dims[dim] // peers, *dims[dim + 1 :])
    return jnp.moveaxis(blocks, dim, 0)


def sum_at_owner(shard, axis, dim):
    peers = lax.axis_size(axis)
    blocks = lax.all_to_all(split_up(shard, dim, peers), axis, 0, 0, tiled=True)
    return jnp.sum(blocks.astype(jnp.float32), axis=0)


def laid_out(blocks, dim):
    blocks = jnp.moveaxis(blocks, 0, dim)
    dims = blocks.shape
    return blocks.reshape(*dims[:dim], dims[dim] * dims[dim + 1], *dims[dim + 2 :])


def gather_directly(shard, axis, dim):
    blocks = from_everyone(shard, axis)
    return laid_out(blocks, dim)


def slot_tables(id_block, gate_block, targets, capacity):
    matches = (id_block[:, :, None] == targets[None, None, :]).astype(jnp.int32)
    per_token = jnp.sum(matches, axis=1)
    earlier = jnp.cumsum(per_token, axis=0) - per_token
    slot_places = lax.broadcasted_iota(jnp.int32, (1, 1, capacity), 2)
    selector = (
        per_token[:, :, None] * (earlier[:, :, None] == slot_places).astype(jnp.int32)
    ).astype(jnp.float32)
    weights = jnp.sum(gate_block[:, :, None] * matches.astype(jnp.float32), axis=1)
    return (selector, weights)


def expert_partial(flat_rows, gate_proj, up_proj, down_proj):
    gate_pre = jnp.minimum(
        jnp.dot(flat_rows, gate_proj[0], preferred_element_type=jnp.float32), CLAMP_LIMIT
    )
    up_pre = jnp.clip(
        jnp.dot(flat_rows, up_proj[0], preferred_element_type=jnp.float32),
        -CLAMP_LIMIT,
        CLAMP_LIMIT,
    )
    activated = ((up_pre + 1.0) * gate_pre * jax.nn.sigmoid(SIGMOID_SLOPE * gate_pre)).astype(
        jnp.bfloat16
    )
    return jnp.dot(activated, down_proj[0], preferred_element_type=jnp.float32)


def local(tokens, norm_gain, expert_ids, route_weights, gate_proj, up_proj, down_proj, final_gain):
    tok_rows, local_width = tokens.shape
    choose_count = expert_ids.shape[1]
    model_width = local_width * lax.axis_size("tp")
    expert_count = lax.axis_size("ep")
    capacity = min(tok_rows, 2 * tok_rows * choose_count // expert_count)
    input_rows = tokens.astype(jnp.float32)
    squares = over_copies(jnp.sum(input_rows * input_rows, axis=1), "tp")
    normed = (
        input_rows * lax.rsqrt(squares / model_width + EPSILON)[:, None] * norm_gain[None, :]
    ).astype(jnp.bfloat16)
    targets = lax.iota(jnp.int32, expert_count)
    selector, weights = slot_tables(expert_ids, route_weights, targets, capacity)
    picker = selector.astype(jnp.bfloat16)
    outbound = jnp.einsum("tec,td->ecd", picker, normed, preferred_element_type=jnp.float32).astype(
        jnp.bfloat16
    )
    received = gather_directly(
        lax.all_to_all(outbound, "ep", split_axis=0, concat_axis=0, tiled=True), "tp", 2
    )
    flat_rows = received.reshape(-1, model_width)
    partial_value = expert_partial(flat_rows, gate_proj, up_proj, down_proj)
    summed = sum_at_owner(partial_value.astype(jnp.bfloat16), "tp", 1).astype(jnp.bfloat16)
    expert_out = summed.reshape(received.shape[0], received.shape[1], local_width)
    returned = lax.all_to_all(expert_out, "ep", split_axis=0, concat_axis=0, tiled=True)
    mixture = jnp.einsum(
        "tec,ecd->td", selector * weights[:, :, None], returned.astype(jnp.float32)
    )
    squares_out = over_copies(jnp.sum(mixture * mixture, axis=1), "tp")
    return (
        mixture * lax.rsqrt(squares_out / model_width + EPSILON)[:, None] * final_gain[None, :]
    ).astype(jnp.bfloat16)


def solution(mesh):
    placed = (
        P("ep", "tp"),
        P("tp"),
        P("ep", None),
        P("ep", None),
        P("ep", None, "tp"),
        P("ep", None, "tp"),
        P("ep", "tp", None),
        P("tp"),
    )
    return jax.shard_map(
        local, mesh=mesh, in_specs=placed, out_specs=P("ep", "tp"), check_vma=False
    )
```

profile of v0, /device:TPU:1, one launch (start us, length us, event | category | flops | bytes accessed | tf_op | source)
XLA Modules:
  0.0 134.4 jit_solution(13776630802675108999)
XLA Ops:
  0.0 0.0 copy-start
  0.0 1.0 fusion.26
  1.0 0.6 broadcast_in_dim.6
  1.6 6.4 %all-to-all-start = ((f32[8,1,64]{2,1,0:T(1,128)}), f32[8,1,64]{2,1,0:T(1,128)S(1)}, u32[]{:S(2)}, u32[]{:S(2)}) async-start(f32[8,1,64]{2,1,0:T(1,128)} %broadcast_in_dim.6), calls=%async_computation | async-start | bytes 8192 | tf_op jit(solution)/shard_map/all_to_all | solution.py:13
  8.0 0.7 convert_reduce_fusion
  8.7 0.1 copy.35
  8.8 0.1 reduce_window_sum.11
  8.9 0.1 copy.37
  9.0 3.5 %all-to-all-done = f32[8,1,64]{2,1,0:T(1,128)S(1)} async-done(((f32[8,1,64]{2,1,0:T(1,128)}), f32[8,1,64]{2,1,0:T(1,128)S(1)}, u32[]{:S(2)}, u32[]{:S(2)}) %all-to-all-start) | async-done | bytes 2080 | tf_op jit(solution)/shard_map/all_to_all | solution.py:13
  12.6 1.0 convolution_convert_fusion.1
  13.6 21.7 %all_to_all.32 = bf16[32,16,256]{2,1,0:T(8,128)(2,1)S(1)} all-to-all(bf16[32,16,256]{2,1,0:T(8,128)(2,1)S(1)} %convolution_convert_fusion.1), channel_id=1, replica_groups=mesh['ep'=32,'tp'=8] {'ep'}, dimensions={0} | all-to-all | bytes 524288 | tf_op jit(solution)/shard_map/all_to_all | solution.py:91
  35.3 0.2 broadcast_in_dim.7
  35.4 31.1 %all_to_all.33 = bf16[8,32,16,256]{3,2,1,0:T(8,128)(2,1)S(1)} all-to-all(bf16[8,32,16,256]{3,2,1,0:T(8,128)(2,1)S(1)} %broadcast_in_dim.7), channel_id=1, replica_groups=mesh['ep'=32,'tp'=8] {'tp'}, dimensions={0} | all-to-all | bytes 4194304 | tf_op jit(solution)/shard_map/all_to_all | solution.py:13
  66.5 1.7 %copy.40 = bf16[32,16,8,256]{3,2,1,0:T(8,128)(2,1)S(1)} copy(bf16[32,16,8,256]{3,1,0,2:T(8,128)(2,1)S(1)} %bitcast.31) | data formatting | bytes 4194304 | tf_op jit(solution)/shard_map/transpose | solution.py:36
  68.2 0.0 copy-start.4
  68.2 0.7 copy.45
  68.9 0.5 copy-done.4
  69.5 1.5 %convolution_minimum_fusion = f32[512,256]{1,0:T(8,128)} fusion(bf16[512,2048]{1,0:T(8,128)(2,1)S(1)} %bitcast.34, bf16[1,2048,256]{2,1,0:T(8,128)(2,1)S(1)} %copy-done.4), kind=kOutput, calls=%fused_computation.2 | convolution fusion | flops 537001984 | bytes 3670016 | tf_op jit(solution)/shard_map/dot_general | solution.py:60
  71.0 0.0 copy-done
  71.0 5.0 %convolution_convert_fusion = bf16[512,2048]{1,0:T(8,128)(2,1)} fusion(f32[512,256]{1,0:T(8,128)} %convolution_minimum_fusion, bf16[512,2048]{1,0:T(8,128)(2,1)S(1)} %bitcast.35, bf16[1,256,2048]{2,1,0:T(8,128)(2,1)S(1)} %copy-done, bf16[1,2048,256]{2,1,0:T(8,128)(2,1)} %param.13), kind=kOutput, calls=%fused_computation | convolution fusion | flops 1075970048 | bytes 6815744 | tf_op jit(solution)/shard_map/dot_general | solution.py:70
  76.0 1.7 %copy.53 = bf16[64,8,8,256]{3,2,0,1:T(8,128)(2,1)S(1)} copy(bf16[64,8,8,256]{3,2,1,0:T(8,128)(2,1)} %bitcast.36) | data formatting | bytes 4194304 | tf_op jit(solution)/shard_map/reshape | solution.py:25
  77.7 29.7 %all_to_all.34 = bf16[8,512,256]{2,1,0:T(8,128)(2,1)S(1)} all-to-all(bf16[8,512,256]{2,1,0:T(8,128)(2,1)S(1)} %bitcast.33), channel_id=1, replica_groups=mesh['ep'=32,'tp'=8] {'tp'}, dimensions={0} | all-to-all | bytes 4194304 | tf_op jit(solution)/shard_map/all_to_all | solution.py:31
  107.4 0.0 copy-start.1
  107.4 0.0 copy-start.2
  107.4 0.0 copy-start.3
  107.4 1.0 reduce_sum.70
  108.4 3.9 %all-to-all-start.4 = ((bf16[32,16,256]{2,1,0:T(8,128)(2,1)}), bf16[32,16,256]{2,1,0:T(8,128)(2,1)S(1)}, u32[]{:S(2)}, u32[]{:S(2)}) async-start(bf16[32,16,256]{2,1,0:T(8,128)(2,1)} %bitcast.7), calls=%async_computation.4 | async-start | bytes 524288 | tf_op jit(solution)/shard_map/all_to_all | solution.py:97
  112.3 0.0 copy-done.1
  112.3 0.0 copy-done.2
  112.3 11.1 %all-to-all-done.4 = bf16[32,16,256]{2,1,0:T(8,128)(2,1)S(1)} async-done(((bf16[32,16,256]{2,1,0:T(8,128)(2,1)}), bf16[32,16,256]{2,1,0:T(8,128)(2,1)S(1)}, u32[]{:S(2)}, u32[]{:S(2)}) %all-to-all-start.4) | async-done | bytes 262176 | tf_op jit(solution)/shard_map/all_to_all | solution.py:97
  123.4 0.3 multiply_reduce_fusion
  123.8 9.9 %all_to_all.35 = f32[8,1,64]{2,1,0:T(1,128)S(1)} all-to-all(f32[8,1,64]{2,1,0:T(1,128)S(1)} %broadcast_in_dim.8), channel_id=1, replica_groups=mesh['ep'=32,'tp'=8] {'tp'}, dimensions={0} | all-to-all | bytes 4096 | tf_op jit(solution)/shard_map/all_to_all | solution.py:13
  133.7 0.0 copy-done.3
  133.7 0.7 multiply_convert_fusion
  (8 shorter events, 0.1 us)
Async XLA Ops:
  0.0 71.0 %copy-start = (bf16[1,256,2048]{2,1,0:T(8,128)(2,1)S(1)}, bf16[1,256,2048]{2,1,0:T(8,128)(2,1)}, u32[]{:S(2)}) copy-start(bf16[1,256,2048]{2,1,0:T(8,128)(2,1)} %param.14) | copy-start | bytes 3145732
  1.6 11.0 %all-to-all-start = ((f32[8,1,64]{2,1,0:T(1,128)}), f32[8,1,64]{2,1,0:T(1,128)S(1)}, u32[]{:S(2)}, u32[]{:S(2)}) async-start(f32[8,1,64]{2,1,0:T(1,128)} %broadcast_in_dim.6), calls=%async_computation | async-start | bytes 8192 | tf_op jit(solution)/shard_map/all_to_all | solution.py:13
  68.2 1.2 copy-start.4
  107.4 4.9 %copy-start.1 = (s32[64,4]{0,1:T(4,128)S(1)}, s32[64,4]{0,1:T(4,128)}, u32[]{:S(2)}) copy-start(s32[64,4]{0,1:T(4,128)} %param.10) | copy-start | bytes 3076
  107.4 4.9 %copy-start.2 = (f32[64,4]{0,1:T(4,128)S(1)}, f32[64,4]{0,1:T(4,128)}, u32[]{:S(2)}) copy-start(f32[64,4]{0,1:T(4,128)} %param.11) | copy-start | bytes 3076
  107.4 26.3 %copy-start.3 = (f32[256]{0:T(256)S(1)}, f32[256]{0:T(256)}, u32[]{:S(2)}) copy-start(f32[256]{0:T(256)} %param.15) | copy-start | bytes 3076
  108.4 15.0 %all-to-all-start.4 = ((bf16[32,16,256]{2,1,0:T(8,128)(2,1)}), bf16[32,16,256]{2,1,0:T(8,128)(2,1)S(1)}, u32[]{:S(2)}, u32[]{:S(2)}) async-start(bf16[32,16,256]{2,1,0:T(8,128)(2,1)} %bitcast.7), calls=%async_computation.4 | async-start | bytes 524288 | tf_op jit(solution)/shard_map/all_to_all | solution.py:97
where the time goes:
time: 135 us; the launch traced here: 134 us
  blocking collectives  92.3 us (68%)
  waiting for transfers between devices  14.6 us (11%)
  starting transfers between devices  10.3 us (8%)
  matrix products  7.92 us (6%)
  local copies, waits for them, and re-layouts  5.61 us (4%)
  other arithmetic  3.59 us (3%)
    all_to_all x2, blocking collectives, from_everyone(): lax.all_to_all(jnp.broadcast_to(shard[None], (peers, *shard.shape)), axis...  41 us
    all_to_all x1, blocking collectives, sum_at_owner(): blocks = lax.all_to_all(split_up(shard, dim, peers), axis, 0, 0, tiled=True)  29.7 us
    all_to_all x1, blocking collectives, local(): lax.all_to_all(outbound, 'ep', split_axis=0, concat_axis=0, tiled=True)  21.7 us
    all_to_all x1, waiting for transfers between devices, local(): lax.all_to_all(expert_out, 'ep', split_axis=0, concat_axis=0, tiled=True)  11.1 us
    all_to_all x1, starting transfers between devices, from_everyone(): lax.all_to_all(jnp.broadcast_to(shard[None], (peers, *shard.shape)), axis...  6.41 us
    dot_general x1, matrix products, expert_partial(): return jnp.dot(activated, down_proj[0], preferred_element_type=jnp.float32)  5.02 us
    all_to_all x1, starting transfers between devices, local(): lax.all_to_all(expert_out, 'ep', split_axis=0, concat_axis=0, tiled=True)  3.87 us
    all_to_all x1, waiting for transfers between devices, from_everyone(): lax.all_to_all(jnp.broadcast_to(shard[None], (peers, *shard.shape)), axis...  3.54 us
  transfers between devices with their start and end apart: 2, of which 2 were waited for; matrix products, arithmetic and copies ran while one was open for 1% of the time, Pallas kernels for 0%

commit v1 on v0

v1 whole, which is shorter than its diff:
```python
import functools

import jax
import jax.numpy as jnp
from jax import lax
from jax.experimental import pallas as pl
from jax.experimental.pallas import tpu as pltpu
from jax.sharding import PartitionSpec as P

MESH = pl.DeviceIdType.MESH
EPSILON = 1e-05
CLAMP_LIMIT = 7.0
SIGMOID_SLOPE = 1.702
F32 = jnp.float32
BF16 = jnp.bfloat16
HIGHEST = lax.Precision.HIGHEST

NZ, NX, NY = 8, 4, 4
N_EP, N_TP = NZ * NX, NY * 2
TOK, CAP, W = 64, 16, 256
D = N_TP * W
K = 4
R = N_EP * CAP // K
PER = N_EP // K


def z_offset(i):
    h = (i + 1) // 2
    return h if i % 2 else (NZ - h) % NZ


def remote(src, dst, send_sem, recv_sem, ep, tp):
    return pltpu.make_async_remote_copy(
        src_ref=src, dst_ref=dst, send_sem=send_sem, recv_sem=recv_sem, device_id=(ep, tp), device_id_type=MESH
    )


def dot(a, b, dims=((1,), (0,)), precision=None):
    return lax.dot_general(a, b, (dims, ((), ())), precision=precision, preferred_element_type=F32)


def kernel(
    tok, ngain, ids, rw, wg_h, wu_h, wd_h, fgain, out,
    wg, wu, wd, gbuf, sbuf, xbuf, ps, q, po, ts, ra, rb, rc, obuf, ybuf, fbuf, wsel,
    wsem, bulk, gsem, a_recv, ag_send, ag_recv, rs_send, rs_recv, y_recv, f_recv,
):
    me_ep, me_tp = lax.axis_index("ep"), lax.axis_index("tp")
    z, x = me_ep // NX, lax.rem(me_ep, NX)
    y, c = me_tp // 2, lax.rem(me_tp, 2)
    d = 1 - 2 * c
    co = 1 - c
    yp, ym, yf = lax.rem(y + d + NY, NY), lax.rem(y - d + NY, NY), lax.rem(y + 2, NY)

    def at(yy, cc):
        return yy * 2 + cc

    def back(p):
        return lax.rem(z - z_offset(p // NX) + NZ, NZ) * NX + lax.rem(x - p % NX + NX, NX)

    def forth(p):
        return lax.rem(z + z_offset(p // NX), NZ) * NX + lax.rem(x + p % NX, NX)

    def peer(i):
        return lax.rem(me_tp + i, N_TP)

    barrier = pltpu.get_barrier_semaphore()
    for p in range(1, N_EP):
        pl.semaphore_signal(barrier, inc=1, device_id=(back(p), me_tp), device_id_type=MESH)
    for i in range(1, N_TP):
        pl.semaphore_signal(barrier, inc=1, device_id=(me_ep, peer(i)), device_id_type=MESH)

    loads = [
        pltpu.make_async_copy(wg_h.at[0], wg, wsem.at[0]),
        pltpu.make_async_copy(wu_h.at[0], wu, wsem.at[1]),
        pltpu.make_async_copy(wd_h.at[0], wd, wsem.at[2]),
    ]
    for load in loads:
        load.start()

    pos = lax.broadcasted_iota(jnp.int32, (TOK, N_EP), 1)
    zi, dx = pos // NX, lax.rem(pos, NX)
    half = (zi + 1) // 2
    dz = jnp.where(lax.rem(zi, 2) == 1, half, NZ - half)
    expert = lax.rem(z - dz + 2 * NZ, NZ) * NX + lax.rem(x - dx + NX, NX)
    match = jnp.zeros((TOK, N_EP), F32)
    weight = jnp.zeros((TOK, N_EP), F32)
    for k in range(ids.shape[1]):
        hit = ids[:, k : k + 1] == expert
        match = match + jnp.where(hit, 1.0, 0.0)
        weight = weight + jnp.where(hit, rw[:, k : k + 1], 0.0)
    before = lax.broadcasted_iota(jnp.int32, (TOK, TOK), 0) > lax.broadcasted_iota(jnp.int32, (TOK, TOK), 1)
    earlier = dot(jnp.where(before, 1.0, 0.0).astype(BF16), match.astype(BF16))
    col = lax.broadcasted_iota(jnp.int32, (N_EP, N_EP * CAP), 1)
    row = lax.broadcasted_iota(jnp.int32, (N_EP, N_EP * CAP), 0)
    spread = jnp.where(col // CAP == row, 1.0, 0.0).astype(BF16)
    slot = lax.rem(lax.broadcasted_iota(jnp.int32, (TOK, N_EP * CAP), 1), CAP).astype(F32)
    taken = (dot(earlier.astype(BF16), spread) == slot) & (dot(match.astype(BF16), spread) > 0.5)
    w_hi = weight.astype(BF16)
    w_lo = (weight - w_hi.astype(F32)).astype(BF16)
    wide = dot(w_hi, spread) + dot(w_lo, spread)
    wsel[...] = jnp.where(taken, wide, 0.0)
    rows = dot(jnp.where(taken, 1.0, 0.0).astype(BF16), tok[...], ((0,), (0,))).astype(BF16)
    sbuf[...] = rows
    xbuf[me_tp, 0:CAP] = rows[0:CAP]
    gbuf[me_tp] = jnp.broadcast_to(ngain[...].reshape(1, W), (8, W))
    pl.semaphore_wait(barrier, N_EP - 1 + N_TP - 1)

    def block(p):
        return pl.ds(p * CAP, CAP)

    def chunk(k):
        return pl.ds(k * R, R)

    for p in range(1, N_EP):
        remote(sbuf.at[block(p)], xbuf.at[me_tp, block(p)], bulk.at[0], a_recv.at[p // PER], back(p), me_tp).start()
    gains = [remote(gbuf.at[me_tp], gbuf.at[me_tp], gsem.at[0, i - 1], gsem.at[1, i - 1], me_ep, peer(i)) for i in range(1, N_TP)]
    for copy in gains:
        copy.start()
    sends = list(gains)

    def send(src, dst, send_sem, recv_sem, tp):
        copy = remote(src, dst, send_sem, recv_sem, me_ep, tp)
        copy.start()
        sends.append(copy)

    def arrived(ref, sem):
        remote(ref, ref, bulk.at[0], sem, me_ep, at(yp, c)).wait_recv()

    def gather_own(k):
        ref = xbuf.at[me_tp, pl.ds(CAP, R - CAP)] if k == 0 else xbuf.at[me_tp, chunk(k)]
        arrived(ref, a_recv.at[k])
        ref = xbuf.at[me_tp, chunk(k)]
        send(ref, ref, ag_send.at[k, 0], ag_recv.at[k, 0], at(yp, c))
        send(ref, ref, ag_send.at[k, 1], ag_recv.at[k, 1], at(ym, c))
        send(ref, ref, ag_send.at[k, 2], ag_recv.at[k, 2], at(y, co))

    def gather_near(k):
        ref = xbuf.at[at(ym, c), chunk(k)]
        arrived(ref, ag_recv.at[k, 0])
        send(ref, ref, ag_send.at[k, 3], ag_recv.at[k, 3], at(yp, c))
        send(ref, ref, ag_send.at[k, 4], ag_recv.at[k, 4], at(y, co))
        ref = xbuf.at[at(yp, c), chunk(k)]
        arrived(ref, ag_recv.at[k, 1])
        send(ref, ref, ag_send.at[k, 5], ag_recv.at[k, 5], at(y, co))

    def gather_far(k):
        ref = xbuf.at[at(yf, c), chunk(k)]
        arrived(ref, ag_recv.at[k, 3])
        send(ref, ref, ag_send.at[k, 6], ag_recv.at[k, 6], at(y, co))

    def compute(k):
        if k == 0:
            for load in loads:
                load.wait()
            for copy in gains:
                copy.wait_recv()
        arrived(xbuf.at[at(y, co), chunk(k)], ag_recv.at[k, 2])
        arrived(xbuf.at[at(yp, co), chunk(k)], ag_recv.at[k, 4])
        arrived(xbuf.at[at(ym, co), chunk(k)], ag_recv.at[k, 5])
        arrived(xbuf.at[at(yf, co), chunk(k)], ag_recv.at[k, 6])
        squares = jnp.zeros((R, W), F32)
        for t in range(N_TP):
            part = xbuf[t, chunk(k)].astype(F32)
            squares = squares + part * part
        scale = lax.rsqrt(jnp.sum(squares, axis=1, keepdims=True) / D + EPSILON)
        gate = jnp.zeros((R, W), F32)
        up = jnp.zeros((R, W), F32)
        for t in range(N_TP):
            part = xbuf[t, chunk(k)].astype(F32)
            normed = (part * scale * gbuf[t, 0:1, :]).astype(BF16)
            gate = gate + dot(normed, wg[t * W : (t + 1) * W, :])
            up = up + dot(normed, wu[t * W : (t + 1) * W, :])
        gate = jnp.minimum(gate, CLAMP_LIMIT)
        up = jnp.clip(up, -CLAMP_LIMIT, CLAMP_LIMIT)
        act = ((up + 1.0) * gate * jax.nn.sigmoid(SIGMOID_SLOPE * gate)).astype(BF16)
        for r in range(NY):
            theirs = at(lax.rem(y - r * d + 2 * NY, NY), co)
            ps[k, r] = dot(act, wd[:, pl.ds(pl.multiple_of(theirs * W, W), W)]).astype(BF16)
        send(ps.at[k], q.at[k], rs_send.at[k, 0], rs_recv.at[k, 0], at(y, co))
        for r in range(NY):
            mine = at(lax.rem(y + r * d + 2 * NY, NY), c)
            po[k, r] = dot(act, wd[:, pl.ds(pl.multiple_of(mine * W, W), W)])

    def pair_sum(k):
        arrived(q.at[k], rs_recv.at[k, 0])
        ts[k, 0] = (po[k, 2] + q[k, 2].astype(F32)).astype(BF16)
        send(ts.at[k, 0], ra.at[k], rs_send.at[k, 1], rs_recv.at[k, 1], at(yp, c))
        ts[k, 1] = (po[k, 3] + q[k, 3].astype(F32)).astype(BF16)
        send(ts.at[k, 1], rb.at[k], rs_send.at[k, 2], rs_recv.at[k, 2], at(ym, c))

    def chain(k):
        arrived(ra.at[k], rs_recv.at[k, 1])
        ts[k, 2] = (po[k, 1] + q[k, 1].astype(F32) + ra[k].astype(F32)).astype(BF16)
        send(ts.at[k, 2], rc.at[k], rs_send.at[k, 3], rs_recv.at[k, 3], at(yp, c))

    def finish(k):
        arrived(rb.at[k], rs_recv.at[k, 2])
        arrived(rc.at[k], rs_recv.at[k, 3])
        total = po[k, 0] + q[k, 0].astype(F32) + rb[k].astype(F32) + rc[k].astype(F32)
        obuf[chunk(k)] = total.astype(BF16)
        if k == 0:
            ybuf[0:CAP] = total[0:CAP].astype(BF16)
        for p in range(max(1, k * PER), (k + 1) * PER):
            remote(obuf.at[block(p)], ybuf.at[block(p)], bulk.at[1], y_recv.at[k], forth(p), me_tp).start()

    stages = [gather_own, gather_near, gather_far, compute, pair_sum, chain, finish]
    for step in range(K + len(stages) - 1):
        for s in reversed(range(len(stages))):
            if 0 <= step - s < K:
                stages[s](step - s)

    mixture = jnp.zeros((TOK, W), F32)
    for k in range(K):
        arrived(ybuf.at[pl.ds(CAP, R - CAP)] if k == 0 else ybuf.at[chunk(k)], y_recv.at[k])
        part = wsel[:, k * R : (k + 1) * R]
        hi = part.astype(BF16)
        lo = (part - hi.astype(F32)).astype(BF16)
        values = ybuf[chunk(k)]
        mixture = mixture + dot(hi, values) + dot(lo, values)
    ones = jnp.ones((8, W), F32)
    sums = dot(ones, mixture * mixture, ((1,), (1,)), HIGHEST)
    fbuf[me_tp] = jnp.concatenate([sums, jnp.zeros((8, 128 - TOK), F32)], axis=1)
    finals = [remote(fbuf.at[me_tp], fbuf.at[me_tp], f_recv.at[0, i - 1], f_recv.at[1, i - 1], me_ep, peer(i)) for i in range(1, N_TP)]
    for copy in finals:
        copy.start()
    for copy in finals:
        copy.wait_recv()
    total = jnp.zeros((8, 128), F32)
    for t in range(N_TP):
        total = total + fbuf[t]
    scale = lax.rsqrt(total / D + EPSILON)
    first = jnp.where(lax.broadcasted_iota(jnp.int32, (8, W), 0) == 0, 1.0, 0.0)
    tall = dot(scale, first, ((0,), (0,)), HIGHEST)[:TOK]
    out[...] = (mixture * tall * fgain[...].reshape(1, W)).astype(BF16)

    for copy in sends + finals:
        copy.wait_send()
    remote(sbuf.at[pl.ds(CAP, N_EP * CAP - CAP)], sbuf.at[pl.ds(CAP, N_EP * CAP - CAP)], bulk.at[0], bulk.at[0], me_ep, at(yp, c)).wait_send()
    remote(obuf.at[pl.ds(CAP, N_EP * CAP - CAP)], obuf.at[pl.ds(CAP, N_EP * CAP - CAP)], bulk.at[1], bulk.at[1], me_ep, at(yp, c)).wait_send()


def step(tokens, norm_gain, expert_ids, route_weights, gate_proj, up_proj, down_proj, final_gain):
    vmem = pl.BlockSpec(memory_space=pltpu.VMEM)
    hbm = pl.BlockSpec(memory_space=pl.ANY)
    rows = N_EP * CAP
    dma = pltpu.SemaphoreType.DMA
    return pl.pallas_call(
        kernel,
        out_shape=jax.ShapeDtypeStruct((TOK, W), BF16),
        in_specs=[vmem, vmem, vmem, vmem, hbm, hbm, hbm, vmem],
        out_specs=vmem,
        scratch_shapes=[
            pltpu.VMEM((D, W), BF16),
            pltpu.VMEM((D, W), BF16),
            pltpu.VMEM((W, D), BF16),
            pltpu.VMEM((N_TP, 8, W), F32),
            pltpu.VMEM((rows, W), BF16),
            pltpu.VMEM((N_TP, rows, W), BF16),
            pltpu.VMEM((K, NY, R, W), BF16),
            pltpu.VMEM((K, NY, R, W), BF16),
            pltpu.VMEM((K, NY, R, W), F32),
            pltpu.VMEM((K, 3, R, W), BF16),
            pltpu.VMEM((K, R, W), BF16),
            pltpu.VMEM((K, R, W), BF16),
            pltpu.VMEM((K, R, W), BF16),
            pltpu.VMEM((rows, W), BF16),
            pltpu.VMEM((rows, W), BF16),
            pltpu.VMEM((N_TP, 8, 128), F32),
            pltpu.VMEM((TOK, rows), F32),
            dma((3,)),
            dma((2,)),
            dma((2, N_TP - 1)),
            dma((K,)),
            dma((K, 7)),
            dma((K, 7)),
            dma((K, 4)),
            dma((K, 4)),
            dma((K,)),
            dma((2, N_TP - 1)),
        ],
        compiler_params=pltpu.CompilerParams(collective_id=0, has_side_effects=True, vmem_limit_bytes=48 * 1024 * 1024),
        name="moe_step",
    )(tokens, norm_gain, expert_ids, route_weights, gate_proj, up_proj, down_proj, final_gain)


def solution(mesh):
    placed = (
        P("ep", "tp"),
        P("tp"),
        P("ep", None),
        P("ep", None),
        P("ep", None, "tp"),
        P("ep", None, "tp"),
        P("ep", "tp", None),
        P("tp"),
    )
    return jax.shard_map(step, mesh=mesh, in_specs=placed, out_specs=P("ep", "tp"), check_vma=False)
```

time: 135 us -> 67.9 us (0.50)
  blocking collectives: 92.3 us -> 0 us
  Pallas kernels: 0 us -> 61.9 us
  waiting for transfers between devices: 14.6 us -> 0 us
  starting transfers between devices: 10.3 us -> 0 us
  matrix products: 7.92 us -> 0 us
  other arithmetic: 3.59 us -> 0 us
    all_to_all x4 -> x0, blocking collectives: 92.3 us -> none  [the longest x2 41 us: from_everyone(): lax.all_to_all(jnp.broadcast_to(shard[None], (peers, *shard.shape)), axis...]
    pallas_call x0 -> x1, Pallas kernels: none -> 61.9 us  [step(): pl.pallas_call(kernel, out_shape=jax.ShapeDtypeStruct((TOK, W), BF16), in...]
    all_to_all x2 -> x0, waiting for transfers between devices: 14.6 us -> none  [the longest x1 11.1 us: local(): lax.all_to_all(expert_out, 'ep', split_axis=0, concat_axis=0, tiled=True)]
    all_to_all x2 -> x0, starting transfers between devices: 10.3 us -> none  [the longest x1 6.41 us: from_everyone(): lax.all_to_all(jnp.broadcast_to(shard[None], (peers, *shard.shape)), axis...]
    dot_general x4 -> x0, matrix products: 7.92 us -> none  [the longest x1 5.02 us: expert_partial(): return jnp.dot(activated, down_proj[0], preferred_element_type=jnp.float32)]
    unnamed x11 -> x17, local copies, waits for them, and re-layouts: 1.23 us -> 5.76 us
    reduce_sum x6 -> x0, other arithmetic: 2.74 us -> none  [the longest x1 1.03 us: sum_at_owner(): return jnp.sum(blocks.astype(jnp.float32), axis=0)]
    reshape x1 -> x0, local copies, waits for them, and re-layouts: 1.73 us -> none  [split_up(): shard.reshape(*dims[:dim], peers, dims[dim] // peers, *dims[dim + 1:])]
  transfers between devices with their start and end apart: 2 -> 0, of which waited for: 2 -> 0; matrix products, arithmetic and copies ran while one was open for 1% -> 0% of each run, Pallas kernels for 0% -> 0%
where the time goes in v1:
time: 67.9 us; the launch traced here: 67.7 us
  Pallas kernels  61.9 us (91%)
  local copies, waits for them, and re-layouts  5.76 us (8%)
    pallas_call x1, Pallas kernels, step(): pl.pallas_call(kernel, out_shape=jax.ShapeDtypeStruct((TOK, W), BF16), in...  61.9 us
    unnamed x17, local copies, waits for them, and re-layouts  5.76 us

profile of v1, /device:TPU:1, one launch (start us, length us, event | category | flops | bytes accessed | tf_op | source)
XLA Modules:
  0.0 67.7 jit_solution(8621813608659191206)
XLA Ops:
  0.0 0.0 copy-start.6
  0.0 0.0 copy-start.3
  0.0 0.8 %copy.9.ids = s32[64,4]{1,0:T(8,128)S(1)} copy(s32[64,4]{0,1:T(4,128)} %param.10) | data formatting | bytes 2048 | tf_op args[2]
  0.8 0.0 copy-done.6
  0.8 0.0 copy-start.4
  0.8 0.0 copy-start.5
  0.8 0.1 copy.10.rw
  0.9 0.0 copy-done.3
  0.9 0.6 copy-done.4
  1.5 0.0 copy-done.5
  1.5 0.0 copy-start
  1.5 1.2 %copy-done = bf16[1,2048,256]{2,1,0:T(8,128)(2,1)S(1)} copy-done((bf16[1,2048,256]{2,1,0:T(8,128)(2,1)S(1)}, bf16[1,2048,256]{2,1,0:T(8,128)(2,1)}, u32[]{:S(2)}) %copy-start) | copy-done | bytes 1048600
  2.7 0.0 copy-start.1
  2.7 1.2 %copy-done.1 = bf16[1,2048,256]{2,1,0:T(8,128)(2,1)S(1)} copy-done((bf16[1,2048,256]{2,1,0:T(8,128)(2,1)S(1)}, bf16[1,2048,256]{2,1,0:T(8,128)(2,1)}, u32[]{:S(2)}) %copy-start.1) | copy-done | bytes 1048600
  3.9 0.0 copy-start.2
  3.9 1.2 %copy-done.2 = bf16[1,256,2048]{2,1,0:T(8,128)(2,1)S(1)} copy-done((bf16[1,256,2048]{2,1,0:T(8,128)(2,1)S(1)}, bf16[1,256,2048]{2,1,0:T(8,128)(2,1)}, u32[]{:S(2)}) %copy-start.2) | copy-done | bytes 1048600
  5.2 61.9 %moe_step.1 = bf16[64,256]{1,0:T(8,128)(2,1)S(1)} custom-call(bf16[64,256]{1,0:T(8,128)(2,1)S(1)} %copy-done.3, f32[256]{0:T(256)S(1)} %copy-done.4, s32[64,4]{1,0:T(8,128)S(1)} %copy.9.ids, f32[64,4]{1,0:T(8,128)S(1)} %copy.10.rw, bf16[1,2048,256]{2,1,0:T(8,128)(2,1)S(1)} %copy-done, bf16[1,2048,256]{2,1,0:T(8,128)(2,1)S(1)} %copy-done.1, ...), custom_call_target="tpu_custom_call" | custom-call | tf_op jit(solution)/shard_map/moe_step/pallas_call | solution.py:247
  67.1 0.6 copy.12
Async XLA Ops:
  0.0 0.8 %copy-start.6 = (f32[64,4]{0,1:T(4,128)S(1)}, f32[64,4]{0,1:T(4,128)}, u32[]{:S(2)}) copy-start(f32[64,4]{0,1:T(4,128)} %param.11) | copy-start | bytes 3076
  0.0 0.9 %copy-start.3 = (bf16[64,256]{1,0:T(8,128)(2,1)S(1)}, bf16[64,256]{1,0:T(8,128)(2,1)}, u32[]{:S(2)}) copy-start(bf16[64,256]{1,0:T(8,128)(2,1)} %tok.1) | copy-start | bytes 98308
  0.8 0.7 %copy-start.4 = (f32[256]{0:T(256)S(1)}, f32[256]{0:T(256)}, u32[]{:S(2)}) copy-start(f32[256]{0:T(256)} %ngain.1) | copy-start | bytes 3076
  0.8 0.7 %copy-start.5 = (f32[256]{0:T(256)S(1)}, f32[256]{0:T(256)}, u32[]{:S(2)}) copy-start(f32[256]{0:T(256)} %fgain.1) | copy-start | bytes 3076
  1.5 1.2 %copy-start = (bf16[1,2048,256]{2,1,0:T(8,128)(2,1)S(1)}, bf16[1,2048,256]{2,1,0:T(8,128)(2,1)}, u32[]{:S(2)}) copy-start(bf16[1,2048,256]{2,1,0:T(8,128)(2,1)} %wg_h.1) | copy-start | bytes 3145732
  2.7 1.2 %copy-start.1 = (bf16[1,2048,256]{2,1,0:T(8,128)(2,1)S(1)}, bf16[1,2048,256]{2,1,0:T(8,128)(2,1)}, u32[]{:S(2)}) copy-start(bf16[1,2048,256]{2,1,0:T(8,128)(2,1)} %wu_h.1) | copy-start | bytes 3145732
  3.9 1.2 %copy-start.2 = (bf16[1,256,2048]{2,1,0:T(8,128)(2,1)S(1)}, bf16[1,256,2048]{2,1,0:T(8,128)(2,1)}, u32[]{:S(2)}) copy-start(bf16[1,256,2048]{2,1,0:T(8,128)(2,1)} %wd_h.1) | copy-start | bytes 3145732

commit v2 on v1

v2 whole, which is shorter than its diff:
```python
import jax
import jax.numpy as jnp
from jax import lax
from jax.experimental import pallas as pl
from jax.experimental.pallas import tpu as pltpu
from jax.sharding import PartitionSpec as P

MESH = pl.DeviceIdType.MESH
EPSILON = 1e-05
CLAMP_LIMIT = 7.0
SIGMOID_SLOPE = 1.702
F32 = jnp.float32
BF16 = jnp.bfloat16
HIGHEST = lax.Precision.HIGHEST

NZ, NX, NY = 8, 4, 4
N_EP, N_TP = NZ * NX, NY * 2
TOK, CAP, W = 64, 16, 256
D = N_TP * W
ROWS = N_EP * CAP
Z_OFFSETS = (2, 3, 4, 5, 6, 1, 7, 0)
NEAR = 5
R = ROWS // NZ
PER = NX
FAR_ROWS = NEAR * R
NEAR_ROWS = ROWS - FAR_ROWS
GROUPS = ((0, 1), (1, 3), (3, 4), (4, 5), (5, 8))
NEAR_GROUP = len(GROUPS) - 1
SELF = PER * Z_OFFSETS.index(0)
ORDER = (
    "S0 o0 o1 o2", "o3 n1 o4 n0", "f0 n2 f1 n3", "f2 m0 C0 f3",
    "C1 n4 f4 C4", "p0 C2 p1 P0", "C3 p2 p3 F1", "F0 F2 F3",
)


def z_offset(i):
    return Z_OFFSETS[i]


def remote(src, dst, send_sem, recv_sem, ep, tp):
    return pltpu.make_async_remote_copy(
        src_ref=src, dst_ref=dst, send_sem=send_sem, recv_sem=recv_sem, device_id=(ep, tp), device_id_type=MESH
    )


def dot(a, b, dims=((1,), (0,)), precision=None):
    return lax.dot_general(a, b, (dims, ((), ())), precision=precision, preferred_element_type=F32)


def kernel(
    tok_h, ngain_h, ids_h, rw_h, wg_h, wu_h, wd_h, fgain_h, out,
    tbuf, ngain, ids, rw, fgain,
    wg, wu, wd, gbuf, sbuf, snear, xbuf, ps, q, po, ts, tn, ra, rb, rc, obuf, ybuf, ynear, mbuf, nbuf, fbuf, wsel, picks,
    wsem, bulk, gsem, t_sem, n_sem, a_recv, ag_send, ag_recv, rs_send, rs_recv, y_recv, f_sem,
):
    me_ep, me_tp = lax.axis_index("ep"), lax.axis_index("tp")
    z, x = me_ep // NX, lax.rem(me_ep, NX)
    y, c = me_tp // 2, lax.rem(me_tp, 2)
    d = 1 - 2 * c
    co = 1 - c
    yp, ym, yf = lax.rem(y + d + NY, NY), lax.rem(y - d + NY, NY), lax.rem(y + 2, NY)

    def at(yy, cc):
        return yy * 2 + cc

    def back(p):
        return lax.rem(z - z_offset(p // NX) + NZ, NZ) * NX + lax.rem(x - p % NX + NX, NX)

    def forth(p):
        return lax.rem(z + z_offset(p // NX), NZ) * NX + lax.rem(x + p % NX, NX)

    def peer(i):
        return lax.rem(me_tp + i, N_TP)

    def hops(p):
        return min(z_offset(p // NX), NZ - z_offset(p // NX)) + min(p % NX, NX - p % NX)

    far = range(NEAR * PER)
    near = [p for p in range(NEAR * PER, N_EP) if p != SELF]
    barrier = pltpu.get_barrier_semaphore()
    for p in sorted([*far, *near], key=lambda p: -hops(p)):
        pl.semaphore_signal(barrier, inc=1, device_id=(back(p), me_tp), device_id_type=MESH)
    for i in range(1, N_TP):
        pl.semaphore_signal(barrier, inc=1, device_id=(me_ep, peer(i)), device_id_type=MESH)

    small = [
        pltpu.make_async_copy(a, b, wsem.at[3 + i])
        for i, (a, b) in enumerate([(ids_h, ids), (rw_h, rw), (tok_h, tbuf.at[y]), (ngain_h, ngain), (fgain_h, fgain)])
    ]
    loads = [
        pltpu.make_async_copy(wg_h.at[0], wg, wsem.at[0]),
        pltpu.make_async_copy(wu_h.at[0], wu, wsem.at[1]),
        pltpu.make_async_copy(wd_h.at[0], wd, wsem.at[2]),
    ]
    for load in small + loads:
        load.start()
    for load in small:
        load.wait()

    pos = lax.broadcasted_iota(jnp.int32, (N_EP, TOK), 0)
    zi, dx = pos // NX, lax.rem(pos, NX)
    dz = jnp.zeros_like(pos)
    for i, offset in enumerate(Z_OFFSETS):
        dz = jnp.where(zi == i, offset, dz)
    expert = lax.rem(z - dz + 2 * NZ, NZ) * NX + lax.rem(x - dx + NX, NX)
    match = jnp.zeros((N_EP, TOK), F32)
    weight = jnp.zeros((N_EP, TOK), F32)
    for k in range(ids.shape[0]):
        hit = ids[k : k + 1, :] == expert
        match = match + jnp.where(hit, 1.0, 0.0)
        weight = weight + jnp.where(hit, rw[k : k + 1, :], 0.0)
    before = lax.broadcasted_iota(jnp.int32, (TOK, TOK), 0) < lax.broadcasted_iota(jnp.int32, (TOK, TOK), 1)
    earlier = dot(match.astype(BF16), jnp.where(before, 1.0, 0.0).astype(BF16))
    row = lax.broadcasted_iota(jnp.int32, (ROWS, N_EP), 0)
    col = lax.broadcasted_iota(jnp.int32, (ROWS, N_EP), 1)
    spread = jnp.where(row // CAP == col, 1.0, 0.0).astype(BF16)
    slot = lax.rem(lax.broadcasted_iota(jnp.int32, (ROWS, TOK), 0), CAP).astype(F32)
    taken = (dot(spread, earlier.astype(BF16)) == slot) & (dot(spread, match.astype(BF16)) > 0.5)
    picks[...] = jnp.where(taken, 1.0, 0.0).astype(BF16)
    sbuf[...] = dot(picks[0:FAR_ROWS], tbuf[y]).astype(BF16)
    gbuf[me_tp] = jnp.broadcast_to(ngain[...], (8, W))
    with jax.named_scope("barrier"):
        pl.semaphore_wait(barrier, N_EP - 1 + N_TP - 1)

    def block(p):
        return pl.ds(p * CAP, CAP)

    def near_block(p):
        return pl.ds(p * CAP - FAR_ROWS, CAP)

    def chunk(k):
        return pl.ds(k * R, R)

    def group(g):
        lo, hi = GROUPS[g]
        return pl.ds(lo * R, (hi - lo) * R)

    all_far = pl.ds(0, FAR_ROWS)
    all_near = pl.ds(FAR_ROWS, NEAR_ROWS)
    own = SELF * CAP - FAR_ROWS
    parts = (pl.ds(0, own), pl.ds(own + CAP, NEAR_ROWS - own - CAP))
    sends = []

    def send(src, dst, send_sem, recv_sem, tp):
        copy = remote(src, dst, send_sem, recv_sem, me_ep, tp)
        copy.start()
        sends.append(copy)

    def arrived(ref, sem):
        remote(ref, ref, bulk.at[0], sem, me_ep, at(yp, c)).wait_recv()

    for i, yy in enumerate((yf, yp, ym)):
        send(tbuf.at[y], tbuf.at[y], t_sem.at[0, i], t_sem.at[1, i], at(yy, c))
    for p in far:
        remote(sbuf.at[block(p)], xbuf.at[y, c, block(p)], bulk.at[0], a_recv.at[p // PER], back(p), me_tp).start()
    gains = []
    for i in range(1, N_TP):
        gains.append(remote(gbuf.at[me_tp], gbuf.at[me_tp], gsem.at[0, i - 1], gsem.at[1, i - 1], me_ep, peer(i)))
        gains[-1].start()
    sends.extend(gains)

    w_hi = weight.astype(BF16)
    w_lo = (weight - w_hi.astype(F32)).astype(BF16)
    chosen = jnp.where(taken, dot(spread, w_hi) + dot(spread, w_lo), 0.0).T
    c_hi = chosen.astype(BF16)
    wsel[0] = c_hi
    wsel[1] = (chosen - c_hi.astype(F32)).astype(BF16)

    def near_dispatch(_):
        for i, yy in enumerate((yf, ym, yp)):
            arrived(tbuf.at[yy], t_sem.at[1, i])
        for yy in range(NY):
            rows = dot(picks[FAR_ROWS:ROWS], tbuf[yy]).astype(BF16)
            snear[yy] = rows
            xbuf[yy, c, SELF * CAP : (SELF + 1) * CAP] = rows[own : own + CAP]
        for p in near:
            i = int(p > SELF)
            remote(snear.at[:, near_block(p)], xbuf.at[:, c, block(p)], bulk.at[1 + i], a_recv.at[NEAR + i], back(p), me_tp).start()

    def near_share(_):
        for i, span in enumerate(parts):
            ref = xbuf.at[:, c, pl.ds(FAR_ROWS + span.start, span.size)]
            arrived(ref, a_recv.at[NEAR + i])
        ref = xbuf.at[:, c, all_near]
        send(ref, ref, ag_send.at[NEAR, 0], ag_recv.at[NEAR, 0], at(y, co))

    def gather_own(k):
        ref = xbuf.at[y, c, chunk(k)]
        arrived(ref, a_recv.at[k])
        send(ref, ref, ag_send.at[k, 3], ag_recv.at[k, 3], at(yf, c))
        send(ref, ref, ag_send.at[k, 0], ag_recv.at[k, 0], at(yp, c))
        send(ref, ref, ag_send.at[k, 1], ag_recv.at[k, 1], at(ym, c))
        send(ref, ref, ag_send.at[k, 2], ag_recv.at[k, 2], at(y, co))

    def gather_near(k):
        ref = xbuf.at[ym, c, chunk(k)]
        arrived(ref, ag_recv.at[k, 0])
        send(ref, ref, ag_send.at[k, 4], ag_recv.at[k, 4], at(y, co))
        ref = xbuf.at[yp, c, chunk(k)]
        arrived(ref, ag_recv.at[k, 1])
        send(ref, ref, ag_send.at[k, 5], ag_recv.at[k, 5], at(y, co))

    def gather_far(k):
        ref = xbuf.at[yf, c, chunk(k)]
        arrived(ref, ag_recv.at[k, 3])
        send(ref, ref, ag_send.at[k, 6], ag_recv.at[k, 6], at(y, co))

    def compute(g):
        if g == 0:
            for load in loads:
                load.wait()
            for copy in gains:
                copy.wait_recv()
        if g == NEAR_GROUP:
            arrived(xbuf.at[:, co, all_near], ag_recv.at[NEAR, 0])
        else:
            for k in range(*GROUPS[g]):
                for i, yy in ((2, y), (4, yp), (5, ym), (6, yf)):
                    arrived(xbuf.at[yy, co, chunk(k)], ag_recv.at[k, i])
        rows = group(g)
        squares = jnp.zeros((rows.size, W), F32)
        for t in range(N_TP):
            part = xbuf[t // 2, t % 2, rows].astype(F32)
            squares = squares + part * part
        scale = lax.rsqrt(jnp.sum(squares, axis=1, keepdims=True) / D + EPSILON)
        gate = jnp.zeros((rows.size, W), F32)
        up = jnp.zeros((rows.size, W), F32)
        for t in range(N_TP):
            part = xbuf[t // 2, t % 2, rows].astype(F32)
            normed = (part * scale * gbuf[t, 0:1, :]).astype(BF16)
            gate = gate + dot(normed, wg[t * W : (t + 1) * W, :])
            up = up + dot(normed, wu[t * W : (t + 1) * W, :])
        gate = jnp.minimum(gate, CLAMP_LIMIT)
        up = jnp.clip(up, -CLAMP_LIMIT, CLAMP_LIMIT)
        act = ((up + 1.0) * gate * jax.nn.sigmoid(SIGMOID_SLOPE * gate)).astype(BF16)
        for yy in range(NY):
            ps[yy, rows] = dot(act, wd[:, pl.ds(pl.multiple_of(at(yy, co) * W, W), W)]).astype(BF16)
        send(ps.at[:, rows], q.at[:, rows], rs_send.at[g, 0], rs_recv.at[g, 0], at(y, co))
        for yy in range(NY):
            po[yy, rows] = dot(act, wd[:, pl.ds(pl.multiple_of(at(yy, c) * W, W), W)])

    def pair(yy, rows):
        return po[yy, rows] + q[yy, rows].astype(F32)

    def pair_sum(g):
        rows = group(g)
        arrived(q.at[:, rows], rs_recv.at[g, 0])
        for i, (yy, ref) in enumerate(((yf, ra), (ym, rb), (yp, rc))):
            ts[i, rows] = pair(yy, rows).astype(BF16)
            send(ts.at[i, rows], ref.at[rows], rs_send.at[g, 1 + i], rs_recv.at[g, 1 + i], at(yy, c))

    def finish(g):
        rows = group(g)
        total = pair(y, rows)
        for i, ref in ((2, rb), (3, rc), (1, ra)):
            arrived(ref.at[rows], rs_recv.at[g, i])
            total = total + ref[rows].astype(F32)
        obuf[rows] = total.astype(BF16)
        for p in range(GROUPS[g][0] * PER, GROUPS[g][1] * PER):
            remote(obuf.at[block(p)], ybuf.at[block(p)], bulk.at[3], y_recv.at[g], forth(p), me_tp).start()

    def near_return(_):
        arrived(q.at[:, all_near], rs_recv.at[NEAR_GROUP, 0])
        for yy in range(NY):
            rows = pair(yy, all_near).astype(BF16)
            tn[yy] = rows
            ynear[yy, own : own + CAP] = rows[own : own + CAP]
        for p in near:
            i = int(p > SELF)
            remote(tn.at[:, near_block(p)], ynear.at[:, near_block(p)], bulk.at[4 + i], y_recv.at[NEAR_GROUP + i], forth(p), me_tp).start()

    def mixed(columns, values):
        return dot(wsel[0, :, columns], values) + dot(wsel[1, :, columns], values)

    stages = dict(
        S=near_dispatch, m=near_share, o=gather_own, n=gather_near, f=gather_far, C=compute, p=pair_sum, F=finish,
        P=near_return,
    )
    for item in " ".join(ORDER).split():
        with jax.named_scope(item):
            stages[item[0]](int(item[1:]))

    with jax.named_scope("near"):
        for i, span in enumerate(parts):
            arrived(ynear.at[:, span], y_recv.at[NEAR_GROUP + i])
    for i, yy in enumerate((yf, yp, ym)):
        mbuf[i] = mixed(slice(FAR_ROWS, ROWS), ynear[yy]).astype(BF16)
        send(mbuf.at[i], nbuf.at[i], n_sem.at[0, i], n_sem.at[1, i], at(yy, c))
    mixture = mixed(slice(FAR_ROWS, ROWS), ynear[y])
    for g in range(NEAR_GROUP):
        with jax.named_scope(f"return{g}"):
            arrived(ybuf.at[group(g)], y_recv.at[g])
        mixture = mixture + mixed(slice(GROUPS[g][0] * R, GROUPS[g][1] * R), ybuf[group(g)])
    with jax.named_scope("near_sum"):
        for i in range(3):
            arrived(nbuf.at[i], n_sem.at[1, i])
    for i in range(3):
        mixture = mixture + nbuf[i].astype(F32)
    ones = jnp.ones((8, W), F32)
    sums = dot(ones, mixture * mixture, ((1,), (1,)), HIGHEST)
    fbuf[me_tp] = jnp.concatenate([sums, jnp.zeros((8, 128 - TOK), F32)], axis=1)
    finals = []
    for i in (4, 3, 5, 2, 6, 7, 1):
        finals.append(remote(fbuf.at[me_tp], fbuf.at[me_tp], f_sem.at[0, i - 1], f_sem.at[1, i - 1], me_ep, peer(i)))
        finals[-1].start()
    with jax.named_scope("final"):
        for copy in finals:
            copy.wait_recv()
    total = jnp.zeros((8, 128), F32)
    for t in range(N_TP):
        total = total + fbuf[t]
    scale = lax.rsqrt(total / D + EPSILON)
    first = jnp.where(lax.broadcasted_iota(jnp.int32, (8, W), 0) == 0, 1.0, 0.0)
    tall = dot(scale, first, ((0,), (0,)), HIGHEST)[:TOK]
    out[...] = (mixture * tall * fgain[...]).astype(BF16)

    with jax.named_scope("drain"):
        for copy in sends + finals:
            copy.wait_send()
        for i, ref in enumerate(
            (sbuf.at[all_far], snear.at[:, parts[0]], snear.at[:, parts[1]], obuf.at[all_far], tn.at[:, parts[0]], tn.at[:, parts[1]])
        ):
            remote(ref, ref, bulk.at[i], bulk.at[i], me_ep, at(yp, c)).wait_send()


def step(tokens, norm_gain, expert_ids, route_weights, gate_proj, up_proj, down_proj, final_gain):
    vmem = pltpu.VMEM
    dma = pltpu.SemaphoreType.DMA
    groups = len(GROUPS)
    return pl.pallas_call(
        kernel,
        out_shape=jax.ShapeDtypeStruct((TOK, W), BF16),
        in_specs=[pl.BlockSpec(memory_space=pltpu.HBM)] * 8,
        out_specs=pl.BlockSpec(memory_space=vmem),
        scratch_shapes=[
            vmem((NY, TOK, W), BF16),
            vmem((1, W), F32),
            vmem((4, TOK), jnp.int32),
            vmem((4, TOK), F32),
            vmem((1, W), F32),
            vmem((D, W), BF16),
            vmem((D, W), BF16),
            vmem((W, D), BF16),
            vmem((N_TP, 8, W), F32),
            vmem((FAR_ROWS, W), BF16),
            vmem((NY, NEAR_ROWS, W), BF16),
            vmem((NY, 2, ROWS, W), BF16),
            vmem((NY, ROWS, W), BF16),
            vmem((NY, ROWS, W), BF16),
            vmem((NY, ROWS, W), F32),
            vmem((3, FAR_ROWS, W), BF16),
            vmem((NY, NEAR_ROWS, W), BF16),
            vmem((FAR_ROWS, W), BF16),
            vmem((FAR_ROWS, W), BF16),
            vmem((FAR_ROWS, W), BF16),
            vmem((FAR_ROWS, W), BF16),
            vmem((FAR_ROWS, W), BF16),
            vmem((NY, NEAR_ROWS, W), BF16),
            vmem((3, TOK, W), BF16),
            vmem((3, TOK, W), BF16),
            vmem((N_TP, 8, 128), F32),
            vmem((2, TOK, ROWS), BF16),
            vmem((ROWS, TOK), BF16),
            dma((8,)),
            dma((6,)),
            dma((2, N_TP - 1)),
            dma((2, 3)),
            dma((2, 3)),
            dma((NEAR + 2,)),
            dma((NEAR + 1, 7)),
            dma((NEAR + 1, 7)),
            dma((groups, 4)),
            dma((groups, 4)),
            dma((groups + 1,)),
            dma((2, N_TP - 1)),
        ],
        compiler_params=pltpu.CompilerParams(collective_id=0, has_side_effects=True, vmem_limit_bytes=50000000),
        name="moe_step",
    )(*[
        pltpu.with_memory_space_constraint(a, pltpu.HBM)
        for a in (tokens, norm_gain.reshape(1, W), expert_ids.T, route_weights.T, gate_proj, up_proj, down_proj, final_gain.reshape(1, W))
    ])


def solution(mesh):
    placed = (
        P("ep", "tp"),
        P("tp"),
        P("ep", None),
        P("ep", None),
        P("ep", None, "tp"),
        P("ep", None, "tp"),
        P("ep", "tp", None),
        P("tp"),
    )
    return jax.shard_map(step, mesh=mesh, in_specs=placed, out_specs=P("ep", "tp"), check_vma=False)
```

time: 67.9 us -> 50.8 us (0.75)
  Pallas kernels: 61.9 us -> 50.1 us
  local copies, waits for them, and re-layouts: 5.76 us -> 0.62 us
    pallas_call x1, Pallas kernels: 61.9 us -> 50.1 us  [step(): pl.pallas_call(kernel, out_shape=jax.ShapeDtypeStruct((TOK, W), BF16), in...]
    unnamed x17 -> x1, local copies, waits for them, and re-layouts: 5.76 us -> 0.62 us
where the time goes in v2:
time: 50.8 us; the launch traced here: 50.7 us
  Pallas kernels  50.1 us (99%)
  local copies, waits for them, and re-layouts  0.62 us (1%)
    pallas_call x1, Pallas kernels, step(): pl.pallas_call(kernel, out_shape=jax.ShapeDtypeStruct((TOK, W), BF16), in...  50.1 us

profile of v2, /device:TPU:1, one launch (start us, length us, event | category | flops | bytes accessed | tf_op | source)
XLA Modules:
  0.0 50.7 jit_solution(13475862407533219841)
XLA Ops:
  0.0 50.1 %moe_step.1 = bf16[64,256]{1,0:T(8,128)(2,1)S(1)} custom-call(bf16[64,256]{1,0:T(8,128)(2,1)} %tok_h.1, f32[1,256]{1,0:T(1,128)} %bitcast.6, s32[4,64]{1,0:T(4,128)} %bitcast.4, f32[4,64]{1,0:T(4,128)} %bitcast.5, bf16[1,2048,256]{2,1,0:T(8,128)(2,1)} %wg_h.1, bf16[1,2048,256]{2,1,0:T(8,128)(2,1)} %wu_h.1, bf16[1,256,2048]{2,1,0:T(8,128)(2,1)} %wd_h.1, ...), custom_call_target="tpu_custom_call" | custom-call | tf_op jit(solution)/shard_map/moe_step/pallas_call | solution.py:330
  50.1 0.6 %copy.10 = bf16[64,256]{1,0:T(8,128)(2,1)} copy(bf16[64,256]{1,0:T(8,128)(2,1)S(1)} %moe_step.1) | data formatting | bytes 65536

commit v3 on v2

--- a/solution.py
+++ b/solution.py
@@ -11,30 +11,32 @@
 SIGMOID_SLOPE = 1.702
 F32 = jnp.float32
 BF16 = jnp.bfloat16
-HIGHEST = lax.Precision.HIGHEST
 
 NZ, NX, NY = 8, 4, 4
 N_EP, N_TP = NZ * NX, NY * 2
 TOK, CAP, W = 64, 16, 256
 D = N_TP * W
 ROWS = N_EP * CAP
-Z_OFFSETS = (2, 3, 4, 5, 6, 1, 7, 0)
+FAR_Z = (2, 6, 3, 5, 4)
+X_OFFSETS = (0, 1, 3, 2)
+NEAR_OFFSETS = (
+    (1, 0), (7, 0), (1, 1), (7, 3),
+    (1, 3), (7, 1), (1, 2), (7, 2),
+    (0, 0), (0, 1), (0, 3), (0, 2),
+)
 NEAR = 5
 R = ROWS // NZ
 PER = NX
 FAR_ROWS = NEAR * R
 NEAR_ROWS = ROWS - FAR_ROWS
-GROUPS = ((0, 1), (1, 3), (3, 4), (4, 5), (5, 8))
+GROUPS = ((0, 1), (1, 2), (2, 3), (3, 4), (4, 5), (5, 8))
 NEAR_GROUP = len(GROUPS) - 1
-SELF = PER * Z_OFFSETS.index(0)
+SELF = PER * NEAR + NEAR_OFFSETS.index((0, 0))
 ORDER = (
-    "S0 o0 o1 o2", "o3 n1 o4 n0", "f0 n2 f1 n3", "f2 m0 C0 f3",
-    "C1 n4 f4 C4", "p0 C2 p1 P0", "C3 p2 p3 F1", "F0 F2 F3",
+    "S0 o0 o1 o2", "n0 f0 o3 o4", "n1 f1 m0 n2", "f2 n3 f3 C5",
+    "n4 f4 C0 C1", "P0 p0 C2 p1", "C3 p2 C4 p3", "F0 p4 F1 F2",
+    "F3 M0 F4",
 )
-
-
-def z_offset(i):
-    return Z_OFFSETS[i]
 
 
 def remote(src, dst, send_sem, recv_sem, ep, tp):
@@ -43,8 +45,8 @@
     )
 
 
-def dot(a, b, dims=((1,), (0,)), precision=None):
-    return lax.dot_general(a, b, (dims, ((), ())), precision=precision, preferred_element_type=F32)
+def dot(a, b, dims=((1,), (0,))):
+    return lax.dot_general(a, b, (dims, ((), ())), preferred_element_type=F32)
 
 
 def kernel(
@@ -63,17 +65,31 @@
     def at(yy, cc):
         return yy * 2 + cc
 
+    def offsets(p):
+        return NEAR_OFFSETS[p - NEAR * PER] if p >= NEAR * PER else (FAR_Z[p // PER], X_OFFSETS[p % PER])
+
     def back(p):
-        return lax.rem(z - z_offset(p // NX) + NZ, NZ) * NX + lax.rem(x - p % NX + NX, NX)
+        dz, dx = offsets(p)
+        return lax.rem(z - dz + NZ, NZ) * NX + lax.rem(x - dx + NX, NX)
 
     def forth(p):
-        return lax.rem(z + z_offset(p // NX), NZ) * NX + lax.rem(x + p % NX, NX)
+        dz, dx = offsets(p)
+        return lax.rem(z + dz, NZ) * NX + lax.rem(x + dx, NX)
+
+    def source(g):
+        return g + 3 * ((g - z + NZ + 1) // NZ) - 1 + (z + NZ - 1) // NZ + (z + 1) // NZ
+
+    def chunk_of(g):
+        past = lax.rem(source(g) - z + NZ, NZ) - 4
+        over, under = (past + NZ - 1) // NZ, (NZ - 1 - past) // NZ
+        return 4 - 2 * past * (over - under) + over
 
     def peer(i):
         return lax.rem(me_tp + i, N_TP)
 
     def hops(p):
-        return min(z_offset(p // NX), NZ - z_offset(p // NX)) + min(p % NX, NX - p % NX)
+        dz, dx = offsets(p)
+        return min(dz, NZ - dz) + min(dx, NX - dx)
 
     far = range(NEAR * PER)
     near = [p for p in range(NEAR * PER, N_EP) if p != SELF]
@@ -98,11 +114,9 @@
         load.wait()
 
     pos = lax.broadcasted_iota(jnp.int32, (N_EP, TOK), 0)
-    zi, dx = pos // NX, lax.rem(pos, NX)
-    dz = jnp.zeros_like(pos)
-    for i, offset in enumerate(Z_OFFSETS):
-        dz = jnp.where(zi == i, offset, dz)
-    expert = lax.rem(z - dz + 2 * NZ, NZ) * NX + lax.rem(x - dx + NX, NX)
+    expert = jnp.zeros_like(pos)
+    for p in range(N_EP):
+        expert = jnp.where(pos == p, back(p), expert)
     match = jnp.zeros((N_EP, TOK), F32)
     weight = jnp.zeros((N_EP, TOK), F32)
     for k in range(ids.shape[0]):
@@ -151,8 +165,16 @@
 
     for i, yy in enumerate((yf, yp, ym)):
         send(tbuf.at[y], tbuf.at[y], t_sem.at[0, i], t_sem.at[1, i], at(yy, c))
-    for p in far:
-        remote(sbuf.at[block(p)], xbuf.at[y, c, block(p)], bulk.at[0], a_recv.at[p // PER], back(p), me_tp).start()
+    def far_dispatch(positions):
+        for p in positions:
+            remote(sbuf.at[block(p)], xbuf.at[y, c, block(p)], bulk.at[0], a_recv.at[p // PER], back(p), me_tp).start()
+
+    far_dispatch(far[: 2 * PER])
+
+    @pl.when(c == 0)
+    def _():
+        far_dispatch(far[2 * PER :])
+
     gains = []
     for i in range(1, N_TP):
         gains.append(remote(gbuf.at[me_tp], gbuf.at[me_tp], gsem.at[0, i - 1], gsem.at[1, i - 1], me_ep, peer(i)))
@@ -167,8 +189,14 @@
     wsel[1] = (chosen - c_hi.astype(F32)).astype(BF16)
 
     def near_dispatch(_):
-        for i, yy in enumerate((yf, ym, yp)):
-            arrived(tbuf.at[yy], t_sem.at[1, i])
+        arrived(tbuf.at[ym], t_sem.at[1, 1])
+
+        @pl.when(c == 1)
+        def _():
+            far_dispatch(far[2 * PER :])
+
+        arrived(tbuf.at[yp], t_sem.at[1, 2])
+        arrived(tbuf.at[yf], t_sem.at[1, 0])
         for yy in range(NY):
             rows = dot(picks[FAR_ROWS:ROWS], tbuf[yy]).astype(BF16)
             snear[yy] = rows
@@ -206,27 +234,28 @@
         send(ref, ref, ag_send.at[k, 6], ag_recv.at[k, 6], at(y, co))
 
     def compute(g):
-        if g == 0:
-            for load in loads:
-                load.wait()
-            for copy in gains:
-                copy.wait_recv()
+        while loads:
+            loads.pop().wait()
+        for copy in gains[:]:
+            copy.wait_recv()
+            gains.remove(copy)
         if g == NEAR_GROUP:
             arrived(xbuf.at[:, co, all_near], ag_recv.at[NEAR, 0])
+            held = all_near
         else:
-            for k in range(*GROUPS[g]):
-                for i, yy in ((2, y), (4, yp), (5, ym), (6, yf)):
-                    arrived(xbuf.at[yy, co, chunk(k)], ag_recv.at[k, i])
+            held = pl.ds(pl.multiple_of(chunk_of(g) * R, R), R)
+            for i, yy in ((2, y), (4, yp), (5, ym), (6, yf)):
+                arrived(xbuf.at[yy, co, held], ag_recv.at[chunk_of(g), i])
         rows = group(g)
         squares = jnp.zeros((rows.size, W), F32)
         for t in range(N_TP):
-            part = xbuf[t // 2, t % 2, rows].astype(F32)
+            part = xbuf[t // 2, t % 2, held].astype(F32)
             squares = squares + part * part
         scale = lax.rsqrt(jnp.sum(squares, axis=1, keepdims=True) / D + EPSILON)
         gate = jnp.zeros((rows.size, W), F32)
         up = jnp.zeros((rows.size, W), F32)
         for t in range(N_TP):
-            part = xbuf[t // 2, t % 2, rows].astype(F32)
+            part = xbuf[t // 2, t % 2, held].astype(F32)
             normed = (part * scale * gbuf[t, 0:1, :]).astype(BF16)
             gate = gate + dot(normed, wg[t * W : (t + 1) * W, :])
             up = up + dot(normed, wu[t * W : (t + 1) * W, :])
@@ -256,8 +285,10 @@
             arrived(ref.at[rows], rs_recv.at[g, i])
             total = total + ref[rows].astype(F32)
         obuf[rows] = total.astype(BF16)
-        for p in range(GROUPS[g][0] * PER, GROUPS[g][1] * PER):
-            remote(obuf.at[block(p)], ybuf.at[block(p)], bulk.at[3], y_recv.at[g], forth(p), me_tp).start()
+        for i, dx in enumerate(X_OFFSETS):
+            place = pl.ds(pl.multiple_of(chunk_of(g) * R + i * CAP, CAP), CAP)
+            device = source(g) * NX + lax.rem(x + dx, NX)
+            remote(obuf.at[block(g * PER + i)], ybuf.at[place], bulk.at[3], y_recv.at[chunk_of(g)], device, me_tp).start()
 
     def near_return(_):
         arrived(q.at[:, all_near], rs_recv.at[NEAR_GROUP, 0])
@@ -267,37 +298,47 @@
             ynear[yy, own : own + CAP] = rows[own : own + CAP]
         for p in near:
             i = int(p > SELF)
-            remote(tn.at[:, near_block(p)], ynear.at[:, near_block(p)], bulk.at[4 + i], y_recv.at[NEAR_GROUP + i], forth(p), me_tp).start()
+            remote(tn.at[:, near_block(p)], ynear.at[:, near_block(p)], bulk.at[4 + i], y_recv.at[NEAR + i], forth(p), me_tp).start()
 
     def mixed(columns, values):
         return dot(wsel[0, :, columns], values) + dot(wsel[1, :, columns], values)
 
+    mixture = []
+
+    def near_mix(_):
+        for i, span in enumerate(parts):
+            arrived(ynear.at[:, span], y_recv.at[NEAR + i])
+        for i, yy in enumerate((yf, yp, ym)):
+            mbuf[i] = mixed(slice(FAR_ROWS, ROWS), ynear[yy]).astype(BF16)
+            send(mbuf.at[i], nbuf.at[i], n_sem.at[0, i], n_sem.at[1, i], at(yy, c))
+        mixture.append(mixed(slice(FAR_ROWS, ROWS), ynear[y]))
+
     stages = dict(
         S=near_dispatch, m=near_share, o=gather_own, n=gather_near, f=gather_far, C=compute, p=pair_sum, F=finish,
-        P=near_return,
+        P=near_return, M=near_mix,
     )
     for item in " ".join(ORDER).split():
         with jax.named_scope(item):
             stages[item[0]](int(item[1:]))
 
-    with jax.named_scope("near"):
-        for i, span in enumerate(parts):
-            arrived(ynear.at[:, span], y_recv.at[NEAR_GROUP + i])
-    for i, yy in enumerate((yf, yp, ym)):
-        mbuf[i] = mixed(slice(FAR_ROWS, ROWS), ynear[yy]).astype(BF16)
-        send(mbuf.at[i], nbuf.at[i], n_sem.at[0, i], n_sem.at[1, i], at(yy, c))
-    mixture = mixed(slice(FAR_ROWS, ROWS), ynear[y])
-    for g in range(NEAR_GROUP):
-        with jax.named_scope(f"return{g}"):
-            arrived(ybuf.at[group(g)], y_recv.at[g])
-        mixture = mixture + mixed(slice(GROUPS[g][0] * R, GROUPS[g][1] * R), ybuf[group(g)])
+    (mixture,) = mixture
+    for k in range(NEAR):
+        with jax.named_scope(f"return{k}"):
+            arrived(ybuf.at[chunk(k)], y_recv.at[k])
+        mixture = mixture + mixed(slice(k * R, (k + 1) * R), ybuf[chunk(k)])
     with jax.named_scope("near_sum"):
         for i in range(3):
             arrived(nbuf.at[i], n_sem.at[1, i])
     for i in range(3):
         mixture = mixture + nbuf[i].astype(F32)
-    ones = jnp.ones((8, W), F32)
-    sums = dot(ones, mixture * mixture, ((1,), (1,)), HIGHEST)
+
+    def halves(a):
+        hi = a.astype(BF16)
+        return hi, (a - hi.astype(F32)).astype(BF16)
+
+    ones = jnp.ones((8, W), BF16)
+    hi, lo = halves(mixture * mixture)
+    sums = dot(ones, hi, ((1,), (1,))) + dot(ones, lo, ((1,), (1,)))
     fbuf[me_tp] = jnp.concatenate([sums, jnp.zeros((8, 128 - TOK), F32)], axis=1)
     finals = []
     for i in (4, 3, 5, 2, 6, 7, 1):
@@ -310,8 +351,9 @@
     for t in range(N_TP):
         total = total + fbuf[t]
     scale = lax.rsqrt(total / D + EPSILON)
-    first = jnp.where(lax.broadcasted_iota(jnp.int32, (8, W), 0) == 0, 1.0, 0.0)
-    tall = dot(scale, first, ((0,), (0,)), HIGHEST)[:TOK]
+    first = jnp.where(lax.broadcasted_iota(jnp.int32, (8, W), 0) == 0, 1.0, 0.0).astype(BF16)
+    hi, lo = halves(scale)
+    tall = (dot(hi, first, ((0,), (0,))) + dot(lo, first, ((0,), (0,))))[:TOK]
     out[...] = (mixture * tall * fgain[...]).astype(BF16)
 
     with jax.named_scope("drain"):
@@ -371,7 +413,7 @@
             dma((NEAR + 1, 7)),
             dma((groups, 4)),
             dma((groups, 4)),
-            dma((groups + 1,)),
+            dma((NEAR + 2,)),
             dma((2, N_TP - 1)),
         ],
         compiler_params=pltpu.CompilerParams(collective_id=0, has_side_effects=True, vmem_limit_bytes=50000000),

time: 50.8 us -> 48.2 us (0.949); the launches traced: 50.7 us -> 47.2 us
  Pallas kernels: 50.1 us -> 46.6 us
    pallas_call x1, Pallas kernels: 50.1 us -> 46.6 us  [step(): pl.pallas_call(kernel, out_shape=jax.ShapeDtypeStruct((TOK, W), BF16), in...]
where the time goes in v3:
time: 48.2 us; the launch traced here: 47.2 us
  Pallas kernels  46.6 us (97%)
  local copies, waits for them, and re-layouts  0.62 us (1%)
    pallas_call x1, Pallas kernels, step(): pl.pallas_call(kernel, out_shape=jax.ShapeDtypeStruct((TOK, W), BF16), in...  46.6 us

profile of v3, /device:TPU:1, one launch (start us, length us, event | category | flops | bytes accessed | tf_op | source)
XLA Modules:
  0.0 47.2 jit_solution(525431877928881211)
XLA Ops:
  0.0 46.6 %moe_step.1 = bf16[64,256]{1,0:T(8,128)(2,1)S(1)} custom-call(bf16[64,256]{1,0:T(8,128)(2,1)} %tok_h.1, f32[1,256]{1,0:T(1,128)} %bitcast.6, s32[4,64]{1,0:T(4,128)} %bitcast.4, f32[4,64]{1,0:T(4,128)} %bitcast.5, bf16[1,2048,256]{2,1,0:T(8,128)(2,1)} %wg_h.1, bf16[1,2048,256]{2,1,0:T(8,128)(2,1)} %wu_h.1, bf16[1,256,2048]{2,1,0:T(8,128)(2,1)} %wd_h.1, ...), custom_call_target="tpu_custom_call" | custom-call | tf_op jit(solution)/shard_map/moe_step/pallas_call | solution.py:372
  46.6 0.6 %copy.10 = bf16[64,256]{1,0:T(8,128)(2,1)} copy(bf16[64,256]{1,0:T(8,128)(2,1)S(1)} %moe_step.1) | data formatting | bytes 65536

commit v4 on v3

--- a/solution.py
+++ b/solution.py
@@ -33,8 +33,8 @@
 NEAR_GROUP = len(GROUPS) - 1
 SELF = PER * NEAR + NEAR_OFFSETS.index((0, 0))
 ORDER = (
-    "S0 o0 o1 o2", "n0 f0 o3 o4", "n1 f1 m0 n2", "f2 n3 f3 C5",
-    "n4 f4 C0 C1", "P0 p0 C2 p1", "C3 p2 C4 p3", "F0 p4 F1 F2",
+    "S0 o0 o1 o2", "n0 f0 o3 o4", "n1 f1 m0 C0", "n2 f2 n3 f3",
+    "C5 p0 n4 f4", "C1 P0 C2 p1", "C3 p2 C4 F0", "p3 p4 F1 F2",
     "F3 M0 F4",
 )
 
@@ -76,8 +76,11 @@
         dz, dx = offsets(p)
         return lax.rem(z + dz, NZ) * NX + lax.rem(x + dx, NX)
 
+    lead = (z - 2) * ((z + NZ - 3) // NZ) * (1 - (z + 2) // NZ)
+
     def source(g):
-        return g + 3 * ((g - z + NZ + 1) // NZ) - 1 + (z + NZ - 1) // NZ + (z + 1) // NZ
+        i = g - 1 + (g - 1 - lead + NZ) // NZ if g else lead
+        return i + 3 * ((i - z + NZ + 1) // NZ) - 1 + (z + NZ - 1) // NZ + (z + 1) // NZ
 
     def chunk_of(g):
         past = lax.rem(source(g) - z + NZ, NZ) - 4

time: 48.2 us -> 47.1 us (0.977)
  Pallas kernels: 46.6 us -> 45.8 us
    pallas_call x1, Pallas kernels: 46.6 us -> 45.8 us  [step(): pl.pallas_call(kernel, out_shape=jax.ShapeDtypeStruct((TOK, W), BF16), in...]
where the time goes in v4:
time: 47.1 us; the launch traced here: 46.4 us
  Pallas kernels  45.8 us (97%)
  local copies, waits for them, and re-layouts  0.62 us (1%)
    pallas_call x1, Pallas kernels, step(): pl.pallas_call(kernel, out_shape=jax.ShapeDtypeStruct((TOK, W), BF16), in...  45.8 us

profile of v4, /device:TPU:1, one launch (start us, length us, event | category | flops | bytes accessed | tf_op | source)
XLA Modules:
  0.0 46.4 jit_solution(12994741628194505645)
XLA Ops:
  0.0 45.8 %moe_step.1 = bf16[64,256]{1,0:T(8,128)(2,1)S(1)} custom-call(bf16[64,256]{1,0:T(8,128)(2,1)} %tok_h.1, f32[1,256]{1,0:T(1,128)} %bitcast.6, s32[4,64]{1,0:T(4,128)} %bitcast.4, f32[4,64]{1,0:T(4,128)} %bitcast.5, bf16[1,2048,256]{2,1,0:T(8,128)(2,1)} %wg_h.1, bf16[1,2048,256]{2,1,0:T(8,128)(2,1)} %wu_h.1, bf16[1,256,2048]{2,1,0:T(8,128)(2,1)} %wd_h.1, ...), custom_call_target="tpu_custom_call" | custom-call | tf_op jit(solution)/shard_map/moe_step/pallas_call | solution.py:375
  45.8 0.6 %copy.10 = bf16[64,256]{1,0:T(8,128)(2,1)} copy(bf16[64,256]{1,0:T(8,128)(2,1)S(1)} %moe_step.1) | data formatting | bytes 65536

commit v5 on v4

--- a/solution.py
+++ b/solution.py
@@ -51,8 +51,8 @@
 
 def kernel(
     tok_h, ngain_h, ids_h, rw_h, wg_h, wu_h, wd_h, fgain_h, out,
-    tbuf, ngain, ids, rw, fgain,
-    wg, wu, wd, gbuf, sbuf, snear, xbuf, ps, q, po, ts, tn, ra, rb, rc, obuf, ybuf, ynear, mbuf, nbuf, fbuf, wsel, picks,
+    tbuf, ids, rw, fgain,
+    wg, wu, wd, gbuf, sbuf, snear, xbuf, ps, q, po, ts, tn, rbuf, obuf, ybuf, ynear, mbuf, nbuf, fbuf, wsel, picks,
     wsem, bulk, gsem, t_sem, n_sem, a_recv, ag_send, ag_recv, rs_send, rs_recv, y_recv, f_sem,
 ):
     me_ep, me_tp = lax.axis_index("ep"), lax.axis_index("tp")
@@ -104,7 +104,7 @@
 
     small = [
         pltpu.make_async_copy(a, b, wsem.at[3 + i])
-        for i, (a, b) in enumerate([(ids_h, ids), (rw_h, rw), (tok_h, tbuf.at[y]), (ngain_h, ngain), (fgain_h, fgain)])
+        for i, (a, b) in enumerate([(ids_h, ids), (rw_h, rw), (tok_h, tbuf.at[y]), (ngain_h, gbuf.at[me_tp]), (fgain_h, fgain)])
     ]
     loads = [
         pltpu.make_async_copy(wg_h.at[0], wg, wsem.at[0]),
@@ -135,7 +135,6 @@
     taken = (dot(spread, earlier.astype(BF16)) == slot) & (dot(spread, match.astype(BF16)) > 0.5)
     picks[...] = jnp.where(taken, 1.0, 0.0).astype(BF16)
     sbuf[...] = dot(picks[0:FAR_ROWS], tbuf[y]).astype(BF16)
-    gbuf[me_tp] = jnp.broadcast_to(ngain[...], (8, W))
     with jax.named_scope("barrier"):
         pl.semaphore_wait(barrier, N_EP - 1 + N_TP - 1)
 
@@ -156,18 +155,14 @@
     all_near = pl.ds(FAR_ROWS, NEAR_ROWS)
     own = SELF * CAP - FAR_ROWS
     parts = (pl.ds(0, own), pl.ds(own + CAP, NEAR_ROWS - own - CAP))
-    sends = []
-
     def send(src, dst, send_sem, recv_sem, tp):
-        copy = remote(src, dst, send_sem, recv_sem, me_ep, tp)
-        copy.start()
-        sends.append(copy)
+        remote(src, dst, send_sem, recv_sem, me_ep, tp).start()
 
     def arrived(ref, sem):
         remote(ref, ref, bulk.at[0], sem, me_ep, at(yp, c)).wait_recv()
 
     for i, yy in enumerate((yf, yp, ym)):
-        send(tbuf.at[y], tbuf.at[y], t_sem.at[0, i], t_sem.at[1, i], at(yy, c))
+        send(tbuf.at[y], tbuf.at[y], t_sem.at[0], t_sem.at[1 + i], at(yy, c))
     def far_dispatch(positions):
         for p in positions:
             remote(sbuf.at[block(p)], xbuf.at[y, c, block(p)], bulk.at[0], a_recv.at[p // PER], back(p), me_tp).start()
@@ -178,11 +173,8 @@
     def _():
         far_dispatch(far[2 * PER :])
 
-    gains = []
     for i in range(1, N_TP):
-        gains.append(remote(gbuf.at[me_tp], gbuf.at[me_tp], gsem.at[0, i - 1], gsem.at[1, i - 1], me_ep, peer(i)))
-        gains[-1].start()
-    sends.extend(gains)
+        send(gbuf.at[me_tp], gbuf.at[me_tp], gsem.at[0], gsem.at[1], peer(i))
 
     w_hi = weight.astype(BF16)
     w_lo = (weight - w_hi.astype(F32)).astype(BF16)
@@ -192,14 +184,14 @@
     wsel[1] = (chosen - c_hi.astype(F32)).astype(BF16)
 
     def near_dispatch(_):
-        arrived(tbuf.at[ym], t_sem.at[1, 1])
+        arrived(tbuf.at[ym], t_sem.at[2])
 
         @pl.when(c == 1)
         def _():
             far_dispatch(far[2 * PER :])
 
-        arrived(tbuf.at[yp], t_sem.at[1, 2])
-        arrived(tbuf.at[yf], t_sem.at[1, 0])
+        arrived(tbuf.at[yp], t_sem.at[3])
+        arrived(tbuf.at[yf], t_sem.at[1])
         for yy in range(NY):
             rows = dot(picks[FAR_ROWS:ROWS], tbuf[yy]).astype(BF16)
             snear[yy] = rows
@@ -213,42 +205,38 @@
             ref = xbuf.at[:, c, pl.ds(FAR_ROWS + span.start, span.size)]
             arrived(ref, a_recv.at[NEAR + i])
         ref = xbuf.at[:, c, all_near]
-        send(ref, ref, ag_send.at[NEAR, 0], ag_recv.at[NEAR, 0], at(y, co))
+        send(ref, ref, ag_send.at[NEAR], ag_recv.at[NEAR, 3], at(y, co))
 
     def gather_own(k):
         ref = xbuf.at[y, c, chunk(k)]
         arrived(ref, a_recv.at[k])
-        send(ref, ref, ag_send.at[k, 3], ag_recv.at[k, 3], at(yf, c))
-        send(ref, ref, ag_send.at[k, 0], ag_recv.at[k, 0], at(yp, c))
-        send(ref, ref, ag_send.at[k, 1], ag_recv.at[k, 1], at(ym, c))
-        send(ref, ref, ag_send.at[k, 2], ag_recv.at[k, 2], at(y, co))
+        for i, tp in ((2, at(yf, c)), (0, at(yp, c)), (1, at(ym, c)), (3, at(y, co))):
+            send(ref, ref, ag_send.at[k], ag_recv.at[k, i], tp)
 
     def gather_near(k):
         ref = xbuf.at[ym, c, chunk(k)]
         arrived(ref, ag_recv.at[k, 0])
-        send(ref, ref, ag_send.at[k, 4], ag_recv.at[k, 4], at(y, co))
+        send(ref, ref, ag_send.at[k], ag_recv.at[k, 3], at(y, co))
         ref = xbuf.at[yp, c, chunk(k)]
         arrived(ref, ag_recv.at[k, 1])
-        send(ref, ref, ag_send.at[k, 5], ag_recv.at[k, 5], at(y, co))
+        send(ref, ref, ag_send.at[k], ag_recv.at[k, 3], at(y, co))
 
     def gather_far(k):
         ref = xbuf.at[yf, c, chunk(k)]
-        arrived(ref, ag_recv.at[k, 3])
-        send(ref, ref, ag_send.at[k, 6], ag_recv.at[k, 6], at(y, co))
+        arrived(ref, ag_recv.at[k, 2])
+        send(ref, ref, ag_send.at[k], ag_recv.at[k, 3], at(y, co))
 
     def compute(g):
+        if loads:
+            arrived(gbuf.at[pl.ds(0, N_TP - 1)], gsem.at[1])
         while loads:
             loads.pop().wait()
-        for copy in gains[:]:
-            copy.wait_recv()
-            gains.remove(copy)
         if g == NEAR_GROUP:
-            arrived(xbuf.at[:, co, all_near], ag_recv.at[NEAR, 0])
+            arrived(xbuf.at[:, co, all_near], ag_recv.at[NEAR, 3])
             held = all_near
         else:
             held = pl.ds(pl.multiple_of(chunk_of(g) * R, R), R)
-            for i, yy in ((2, y), (4, yp), (5, ym), (6, yf)):
-                arrived(xbuf.at[yy, co, held], ag_recv.at[chunk_of(g), i])
+            arrived(xbuf.at[:, co, held], ag_recv.at[chunk_of(g), 3])
         rows = group(g)
         squares = jnp.zeros((rows.size, W), F32)
         for t in range(N_TP):
@@ -259,7 +247,7 @@
         up = jnp.zeros((rows.size, W), F32)
         for t in range(N_TP):
             part = xbuf[t // 2, t % 2, held].astype(F32)
-            normed = (part * scale * gbuf[t, 0:1, :]).astype(BF16)
+            normed = (part * scale * gbuf[t]).astype(BF16)
             gate = gate + dot(normed, wg[t * W : (t + 1) * W, :])
             up = up + dot(normed, wu[t * W : (t + 1) * W, :])
         gate = jnp.minimum(gate, CLAMP_LIMIT)
@@ -267,7 +255,7 @@
         act = ((up + 1.0) * gate * jax.nn.sigmoid(SIGMOID_SLOPE * gate)).astype(BF16)
         for yy in range(NY):
             ps[yy, rows] = dot(act, wd[:, pl.ds(pl.multiple_of(at(yy, co) * W, W), W)]).astype(BF16)
-        send(ps.at[:, rows], q.at[:, rows], rs_send.at[g, 0], rs_recv.at[g, 0], at(y, co))
+        send(ps.at[:, rows], q.at[:, rows], rs_send.at[g], rs_recv.at[g, 0], at(y, co))
         for yy in range(NY):
             po[yy, rows] = dot(act, wd[:, pl.ds(pl.multiple_of(at(yy, c) * W, W), W)])
 
@@ -277,16 +265,16 @@
     def pair_sum(g):
         rows = group(g)
         arrived(q.at[:, rows], rs_recv.at[g, 0])
-        for i, (yy, ref) in enumerate(((yf, ra), (ym, rb), (yp, rc))):
+        for i, yy in enumerate((yf, ym, yp)):
             ts[i, rows] = pair(yy, rows).astype(BF16)
-            send(ts.at[i, rows], ref.at[rows], rs_send.at[g, 1 + i], rs_recv.at[g, 1 + i], at(yy, c))
+            send(ts.at[i, rows], rbuf.at[i, rows], rs_send.at[g], rs_recv.at[g, 1], at(yy, c))
 
     def finish(g):
         rows = group(g)
         total = pair(y, rows)
-        for i, ref in ((2, rb), (3, rc), (1, ra)):
-            arrived(ref.at[rows], rs_recv.at[g, i])
-            total = total + ref[rows].astype(F32)
+        arrived(rbuf.at[:, rows], rs_recv.at[g, 1])
+        for i in range(3):
+            total = total + rbuf[i, rows].astype(F32)
         obuf[rows] = total.astype(BF16)
         for i, dx in enumerate(X_OFFSETS):
             place = pl.ds(pl.multiple_of(chunk_of(g) * R + i * CAP, CAP), CAP)
@@ -313,7 +301,7 @@
             arrived(ynear.at[:, span], y_recv.at[NEAR + i])
         for i, yy in enumerate((yf, yp, ym)):
             mbuf[i] = mixed(slice(FAR_ROWS, ROWS), ynear[yy]).astype(BF16)
-            send(mbuf.at[i], nbuf.at[i], n_sem.at[0, i], n_sem.at[1, i], at(yy, c))
+            send(mbuf.at[i], nbuf.at[i], n_sem.at[0], n_sem.at[1], at(yy, c))
         mixture.append(mixed(slice(FAR_ROWS, ROWS), ynear[y]))
 
     stages = dict(
@@ -330,8 +318,7 @@
             arrived(ybuf.at[chunk(k)], y_recv.at[k])
         mixture = mixture + mixed(slice(k * R, (k + 1) * R), ybuf[chunk(k)])
     with jax.named_scope("near_sum"):
-        for i in range(3):
-            arrived(nbuf.at[i], n_sem.at[1, i])
+        arrived(nbuf, n_sem.at[1])
     for i in range(3):
         mixture = mixture + nbuf[i].astype(F32)
 
@@ -342,30 +329,30 @@
     ones = jnp.ones((8, W), BF16)
     hi, lo = halves(mixture * mixture)
     sums = dot(ones, hi, ((1,), (1,))) + dot(ones, lo, ((1,), (1,)))
-    fbuf[me_tp] = jnp.concatenate([sums, jnp.zeros((8, 128 - TOK), F32)], axis=1)
-    finals = []
+    fbuf[me_tp] = jnp.concatenate([sums, jnp.zeros((8, 128 - TOK), F32)], axis=1)[0:1]
     for i in (4, 3, 5, 2, 6, 7, 1):
-        finals.append(remote(fbuf.at[me_tp], fbuf.at[me_tp], f_sem.at[0, i - 1], f_sem.at[1, i - 1], me_ep, peer(i)))
-        finals[-1].start()
+        send(fbuf.at[me_tp], fbuf.at[me_tp], f_sem.at[0], f_sem.at[1], peer(i))
     with jax.named_scope("final"):
-        for copy in finals:
-            copy.wait_recv()
-    total = jnp.zeros((8, 128), F32)
+        arrived(fbuf.at[pl.ds(0, N_TP - 1)], f_sem.at[1])
+    total = jnp.zeros((1, 128), F32)
     for t in range(N_TP):
         total = total + fbuf[t]
-    scale = lax.rsqrt(total / D + EPSILON)
+    scale = jnp.broadcast_to(lax.rsqrt(total / D + EPSILON), (8, 128))
     first = jnp.where(lax.broadcasted_iota(jnp.int32, (8, W), 0) == 0, 1.0, 0.0).astype(BF16)
     hi, lo = halves(scale)
     tall = (dot(hi, first, ((0,), (0,))) + dot(lo, first, ((0,), (0,))))[:TOK]
     out[...] = (mixture * tall * fgain[...]).astype(BF16)
 
+    seven = xbuf.at[0, 0, pl.ds(0, 7 * R)]
+    sent = [(seven, ag_send.at[k]) for k in range(NEAR)] + [(seven, rs_send.at[g]) for g in range(NEAR_GROUP)]
+    sent += [(q.at[:, all_near], ag_send.at[NEAR]), (q.at[:, all_near], rs_send.at[NEAR_GROUP])]
+    sent += [(gbuf.at[pl.ds(0, N_TP - 1)], gsem.at[0]), (fbuf.at[pl.ds(0, N_TP - 1)], f_sem.at[0])]
+    sent += [(tbuf.at[pl.ds(0, 3)], t_sem.at[0]), (mbuf, n_sem.at[0]), (sbuf.at[all_far], bulk.at[0]), (obuf.at[all_far], bulk.at[3])]
+    for i, span in enumerate(parts):
+        sent += [(snear.at[:, span], bulk.at[1 + i]), (tn.at[:, span], bulk.at[4 + i])]
     with jax.named_scope("drain"):
-        for copy in sends + finals:
-            copy.wait_send()
-        for i, ref in enumerate(
-            (sbuf.at[all_far], snear.at[:, parts[0]], snear.at[:, parts[1]], obuf.at[all_far], tn.at[:, parts[0]], tn.at[:, parts[1]])
-        ):
-            remote(ref, ref, bulk.at[i], bulk.at[i], me_ep, at(yp, c)).wait_send()
+        for ref, sem in sent:
+            remote(ref, ref, sem, sem, me_ep, at(yp, c)).wait_send()
 
 
 def step(tokens, norm_gain, expert_ids, route_weights, gate_proj, up_proj, down_proj, final_gain):
@@ -379,14 +366,13 @@
         out_specs=pl.BlockSpec(memory_space=vmem),
         scratch_shapes=[
             vmem((NY, TOK, W), BF16),
-            vmem((1, W), F32),
             vmem((4, TOK), jnp.int32),
             vmem((4, TOK), F32),
             vmem((1, W), F32),
             vmem((D, W), BF16),
             vmem((D, W), BF16),
             vmem((W, D), BF16),
-            vmem((N_TP, 8, W), F32),
+            vmem((N_TP, 1, W), F32),
             vmem((FAR_ROWS, W), BF16),
             vmem((NY, NEAR_ROWS, W), BF16),
             vmem((NY, 2, ROWS, W), BF16),
@@ -395,29 +381,27 @@
             vmem((NY, ROWS, W), F32),
             vmem((3, FAR_ROWS, W), BF16),
             vmem((NY, NEAR_ROWS, W), BF16),
-            vmem((FAR_ROWS, W), BF16),
-            vmem((FAR_ROWS, W), BF16),
-            vmem((FAR_ROWS, W), BF16),
+            vmem((3, FAR_ROWS, W), BF16),
             vmem((FAR_ROWS, W), BF16),
             vmem((FAR_ROWS, W), BF16),
             vmem((NY, NEAR_ROWS, W), BF16),
             vmem((3, TOK, W), BF16),
             vmem((3, TOK, W), BF16),
-            vmem((N_TP, 8, 128), F32),
+            vmem((N_TP, 1, 128), F32),
             vmem((2, TOK, ROWS), BF16),
             vmem((ROWS, TOK), BF16),
             dma((8,)),
             dma((6,)),
-            dma((2, N_TP - 1)),
-            dma((2, 3)),
-            dma((2, 3)),
+            dma((2,)),
+            dma((4,)),
+            dma((2,)),
             dma((NEAR + 2,)),
-            dma((NEAR + 1, 7)),
-            dma((NEAR + 1, 7)),
-            dma((groups, 4)),
-            dma((groups, 4)),
+            dma((NEAR + 1,)),
+            dma((NEAR + 1, 4)),
+            dma((groups,)),
+            dma((groups, 2)),
             dma((NEAR + 2,)),
-            dma((2, N_TP - 1)),
+            dma((2,)),
         ],
         compiler_params=pltpu.CompilerParams(collective_id=0, has_side_effects=True, vmem_limit_bytes=50000000),
         name="moe_step",

time: 47.1 us -> 45.9 us (0.975)
  Pallas kernels: 45.8 us -> 44.4 us
    pallas_call x1, Pallas kernels: 45.8 us -> 44.4 us  [step(): pl.pallas_call(kernel, out_shape=jax.ShapeDtypeStruct((TOK, W), BF16), in...]
where the time goes in v5:
time: 45.9 us; the launch traced here: 45 us
  Pallas kernels  44.4 us (97%)
  local copies, waits for them, and re-layouts  0.62 us (1%)
    pallas_call x1, Pallas kernels, step(): pl.pallas_call(kernel, out_shape=jax.ShapeDtypeStruct((TOK, W), BF16), in...  44.4 us

profile of v5, /device:TPU:1, one launch (start us, length us, event | category | flops | bytes accessed | tf_op | source)
XLA Modules:
  0.0 45.0 jit_solution(9245905830799014295)
XLA Ops:
  0.0 44.4 %moe_step.1 = bf16[64,256]{1,0:T(8,128)(2,1)S(1)} custom-call(bf16[64,256]{1,0:T(8,128)(2,1)} %tok_h.1, f32[1,256]{1,0:T(1,128)} %bitcast.6, s32[4,64]{1,0:T(4,128)} %bitcast.4, f32[4,64]{1,0:T(4,128)} %bitcast.5, bf16[1,2048,256]{2,1,0:T(8,128)(2,1)} %wg_h.1, bf16[1,2048,256]{2,1,0:T(8,128)(2,1)} %wu_h.1, bf16[1,256,2048]{2,1,0:T(8,128)(2,1)} %wd_h.1, ...), custom_call_target="tpu_custom_call" | custom-call | tf_op jit(solution)/shard_map/moe_step/pallas_call | solution.py:362
  44.4 0.6 %copy.10 = bf16[64,256]{1,0:T(8,128)(2,1)} copy(bf16[64,256]{1,0:T(8,128)(2,1)S(1)} %moe_step.1) | data formatting | bytes 65536

commit v6 on v5

--- a/solution.py
+++ b/solution.py
@@ -198,33 +198,33 @@
             xbuf[yy, c, SELF * CAP : (SELF + 1) * CAP] = rows[own : own + CAP]
         for p in near:
             i = int(p > SELF)
-            remote(snear.at[:, near_block(p)], xbuf.at[:, c, block(p)], bulk.at[1 + i], a_recv.at[NEAR + i], back(p), me_tp).start()
+            remote(snear.at[:, near_block(p)], xbuf.at[:, c, block(p)], bulk.at[0], a_recv.at[NEAR + i], back(p), me_tp).start()
 
     def near_share(_):
         for i, span in enumerate(parts):
             ref = xbuf.at[:, c, pl.ds(FAR_ROWS + span.start, span.size)]
             arrived(ref, a_recv.at[NEAR + i])
         ref = xbuf.at[:, c, all_near]
-        send(ref, ref, ag_send.at[NEAR], ag_recv.at[NEAR, 3], at(y, co))
+        send(ref, ref, ag_send.at[0], ag_recv.at[NEAR, 3], at(y, co))
 
     def gather_own(k):
         ref = xbuf.at[y, c, chunk(k)]
         arrived(ref, a_recv.at[k])
         for i, tp in ((2, at(yf, c)), (0, at(yp, c)), (1, at(ym, c)), (3, at(y, co))):
-            send(ref, ref, ag_send.at[k], ag_recv.at[k, i], tp)
+            send(ref, ref, ag_send.at[0], ag_recv.at[k, i], tp)
 
     def gather_near(k):
         ref = xbuf.at[ym, c, chunk(k)]
         arrived(ref, ag_recv.at[k, 0])
-        send(ref, ref, ag_send.at[k], ag_recv.at[k, 3], at(y, co))
+        send(ref, ref, ag_send.at[0], ag_recv.at[k, 3], at(y, co))
         ref = xbuf.at[yp, c, chunk(k)]
         arrived(ref, ag_recv.at[k, 1])
-        send(ref, ref, ag_send.at[k], ag_recv.at[k, 3], at(y, co))
+        send(ref, ref, ag_send.at[0], ag_recv.at[k, 3], at(y, co))
 
     def gather_far(k):
         ref = xbuf.at[yf, c, chunk(k)]
         arrived(ref, ag_recv.at[k, 2])
-        send(ref, ref, ag_send.at[k], ag_recv.at[k, 3], at(y, co))
+        send(ref, ref, ag_send.at[0], ag_recv.at[k, 3], at(y, co))
 
     def compute(g):
         if loads:
@@ -255,7 +255,7 @@
         act = ((up + 1.0) * gate * jax.nn.sigmoid(SIGMOID_SLOPE * gate)).astype(BF16)
         for yy in range(NY):
             ps[yy, rows] = dot(act, wd[:, pl.ds(pl.multiple_of(at(yy, co) * W, W), W)]).astype(BF16)
-        send(ps.at[:, rows], q.at[:, rows], rs_send.at[g], rs_recv.at[g, 0], at(y, co))
+        send(ps.at[:, rows], q.at[:, rows], rs_send.at[0], rs_recv.at[g, 0], at(y, co))
         for yy in range(NY):
             po[yy, rows] = dot(act, wd[:, pl.ds(pl.multiple_of(at(yy, c) * W, W), W)])
 
@@ -267,7 +267,7 @@
         arrived(q.at[:, rows], rs_recv.at[g, 0])
         for i, yy in enumerate((yf, ym, yp)):
             ts[i, rows] = pair(yy, rows).astype(BF16)
-            send(ts.at[i, rows], rbuf.at[i, rows], rs_send.at[g], rs_recv.at[g, 1], at(yy, c))
+            send(ts.at[i, rows], rbuf.at[i, rows], rs_send.at[0], rs_recv.at[g, 1], at(yy, c))
 
     def finish(g):
         rows = group(g)
@@ -279,7 +279,7 @@
         for i, dx in enumerate(X_OFFSETS):
             place = pl.ds(pl.multiple_of(chunk_of(g) * R + i * CAP, CAP), CAP)
             device = source(g) * NX + lax.rem(x + dx, NX)
-            remote(obuf.at[block(g * PER + i)], ybuf.at[place], bulk.at[3], y_recv.at[chunk_of(g)], device, me_tp).start()
+            remote(obuf.at[block(g * PER + i)], ybuf.at[place], bulk.at[0], y_recv.at[chunk_of(g)], device, me_tp).start()
 
     def near_return(_):
         arrived(q.at[:, all_near], rs_recv.at[NEAR_GROUP, 0])
@@ -289,7 +289,7 @@
             ynear[yy, own : own + CAP] = rows[own : own + CAP]
         for p in near:
             i = int(p > SELF)
-            remote(tn.at[:, near_block(p)], ynear.at[:, near_block(p)], bulk.at[4 + i], y_recv.at[NEAR + i], forth(p), me_tp).start()
+            remote(tn.at[:, near_block(p)], ynear.at[:, near_block(p)], bulk.at[0], y_recv.at[NEAR + i], forth(p), me_tp).start()
 
     def mixed(columns, values):
         return dot(wsel[0, :, columns], values) + dot(wsel[1, :, columns], values)
@@ -343,13 +343,9 @@
     tall = (dot(hi, first, ((0,), (0,))) + dot(lo, first, ((0,), (0,))))[:TOK]
     out[...] = (mixture * tall * fgain[...]).astype(BF16)
 
-    seven = xbuf.at[0, 0, pl.ds(0, 7 * R)]
-    sent = [(seven, ag_send.at[k]) for k in range(NEAR)] + [(seven, rs_send.at[g]) for g in range(NEAR_GROUP)]
-    sent += [(q.at[:, all_near], ag_send.at[NEAR]), (q.at[:, all_near], rs_send.at[NEAR_GROUP])]
-    sent += [(gbuf.at[pl.ds(0, N_TP - 1)], gsem.at[0]), (fbuf.at[pl.ds(0, N_TP - 1)], f_sem.at[0])]
-    sent += [(tbuf.at[pl.ds(0, 3)], t_sem.at[0]), (mbuf, n_sem.at[0]), (sbuf.at[all_far], bulk.at[0]), (obuf.at[all_far], bulk.at[3])]
-    for i, span in enumerate(parts):
-        sent += [(snear.at[:, span], bulk.at[1 + i]), (tn.at[:, span], bulk.at[4 + i])]
+    gathered = po.at[:, pl.ds(0, (7 * FAR_ROWS + NY * NEAR_ROWS) // (2 * NY))]
+    sent = [(gathered, ag_send.at[0]), (gathered, rs_send.at[0]), (q, bulk.at[0]), (tbuf.at[pl.ds(0, 3)], t_sem.at[0])]
+    sent += [(gbuf.at[pl.ds(0, N_TP - 1)], gsem.at[0]), (fbuf.at[pl.ds(0, N_TP - 1)], f_sem.at[0]), (mbuf, n_sem.at[0])]
     with jax.named_scope("drain"):
         for ref, sem in sent:
             remote(ref, ref, sem, sem, me_ep, at(yp, c)).wait_send()
@@ -391,14 +387,14 @@
             vmem((2, TOK, ROWS), BF16),
             vmem((ROWS, TOK), BF16),
             dma((8,)),
-            dma((6,)),
+            dma((1,)),
             dma((2,)),
             dma((4,)),
             dma((2,)),
             dma((NEAR + 2,)),
-            dma((NEAR + 1,)),
+            dma((1,)),
             dma((NEAR + 1, 4)),
-            dma((groups,)),
+            dma((1,)),
             dma((groups, 2)),
             dma((NEAR + 2,)),
             dma((2,)),

time: 45.9 us -> 45.8 us (level)
  no operation moved by 1% of the time
where the time goes in v6:
time: 45.8 us; the launch traced here: 44.9 us
  Pallas kernels  44.2 us (97%)
  local copies, waits for them, and re-layouts  0.62 us (1%)
    pallas_call x1, Pallas kernels, step(): pl.pallas_call(kernel, out_shape=jax.ShapeDtypeStruct((TOK, W), BF16), in...  44.2 us

profile of v6, /device:TPU:1, one launch (start us, length us, event | category | flops | bytes accessed | tf_op | source)
XLA Modules:
  0.0 44.9 jit_solution(8080454126901984497)
XLA Ops:
  0.0 44.2 %moe_step.1 = bf16[64,256]{1,0:T(8,128)(2,1)S(1)} custom-call(bf16[64,256]{1,0:T(8,128)(2,1)} %tok_h.1, f32[1,256]{1,0:T(1,128)} %bitcast.6, s32[4,64]{1,0:T(4,128)} %bitcast.4, f32[4,64]{1,0:T(4,128)} %bitcast.5, bf16[1,2048,256]{2,1,0:T(8,128)(2,1)} %wg_h.1, bf16[1,2048,256]{2,1,0:T(8,128)(2,1)} %wu_h.1, bf16[1,256,2048]{2,1,0:T(8,128)(2,1)} %wd_h.1, ...), custom_call_target="tpu_custom_call" | custom-call | tf_op jit(solution)/shard_map/moe_step/pallas_call | solution.py:358
  44.3 0.6 %copy.10 = bf16[64,256]{1,0:T(8,128)(2,1)} copy(bf16[64,256]{1,0:T(8,128)(2,1)S(1)} %moe_step.1) | data formatting | bytes 65536

commit v7 on v6

--- a/solution.py
+++ b/solution.py
@@ -326,10 +326,9 @@
         hi = a.astype(BF16)
         return hi, (a - hi.astype(F32)).astype(BF16)
 
-    ones = jnp.ones((8, W), BF16)
-    hi, lo = halves(mixture * mixture)
-    sums = dot(ones, hi, ((1,), (1,))) + dot(ones, lo, ((1,), (1,)))
-    fbuf[me_tp] = jnp.concatenate([sums, jnp.zeros((8, 128 - TOK), F32)], axis=1)[0:1]
+    sums = jnp.sum(mixture * mixture, axis=1, keepdims=True)
+    sums = jnp.broadcast_to(jnp.concatenate([sums, jnp.zeros((128 - TOK, 1), F32)], axis=0), (128, 128))
+    fbuf[me_tp] = sums.T[0:1]
     for i in (4, 3, 5, 2, 6, 7, 1):
         send(fbuf.at[me_tp], fbuf.at[me_tp], f_sem.at[0], f_sem.at[1], peer(i))
     with jax.named_scope("final"):

time: 45.8 us -> 45.8 us (level)
  no operation moved by 1% of the time
where the time goes in v7:
time: 45.8 us; the launch traced here: 44.9 us
  Pallas kernels  44.3 us (97%)
  local copies, waits for them, and re-layouts  0.62 us (1%)
    pallas_call x1, Pallas kernels, step(): pl.pallas_call(kernel, out_shape=jax.ShapeDtypeStruct((TOK, W), BF16), in...  44.3 us

profile of v7, /device:TPU:1, one launch (start us, length us, event | category | flops | bytes accessed | tf_op | source)
XLA Modules:
  0.0 44.9 jit_solution(15352060292934595771)
XLA Ops:
  0.0 44.3 %moe_step.1 = bf16[64,256]{1,0:T(8,128)(2,1)S(1)} custom-call(bf16[64,256]{1,0:T(8,128)(2,1)} %tok_h.1, f32[1,256]{1,0:T(1,128)} %bitcast.6, s32[4,64]{1,0:T(4,128)} %bitcast.4, f32[4,64]{1,0:T(4,128)} %bitcast.5, bf16[1,2048,256]{2,1,0:T(8,128)(2,1)} %wg_h.1, bf16[1,2048,256]{2,1,0:T(8,128)(2,1)} %wu_h.1, bf16[1,256,2048]{2,1,0:T(8,128)(2,1)} %wd_h.1, ...), custom_call_target="tpu_custom_call" | custom-call | tf_op jit(solution)/shard_map/moe_step/pallas_call | solution.py:357
  44.3 0.6 %copy.10 = bf16[64,256]{1,0:T(8,128)(2,1)} copy(bf16[64,256]{1,0:T(8,128)(2,1)S(1)} %moe_step.1) | data formatting | bytes 65536
